TPU v7x, 512 devices: a whole 4x8x8 slice. The times are simulated.
512 devices in a mesh: ep: 32 (over z, x), tp: 16 (over y, core).
Axes of the slice: x: 4, y: 8, z: 8, core: 2. Of those that a mesh axis runs over, the one named last changes fastest.
Arguments:
- mix_input: bfloat16 [16384, 2048], P('ep', 'tp'), may hold values from -6 to 6
- mix_weight: bfloat16 [2048, 4096], P(None, 'tp'), may hold values from -0.125 to 0.125
- expert_input: bfloat16 [4096, 4096], P('ep', 'tp'), may hold values from -4500 to 4500
- expert_index: int32 [4096, 2], P('ep'), may hold values from 0 to 31, as said below
- route_share: float32 [4096, 2], P('ep'), may hold values from 0.1 to 1
- norm_gain: float32 [4096], replicated, may hold values from 0.1 to 1.9
- gate_weight: bfloat16 [32, 4096, 2048], P('ep', None, 'tp'), may hold values from -0.09375 to 0.09375
- up_weight: bfloat16 [32, 4096, 2048], P('ep', None, 'tp'), may hold values from -0.09375 to 0.09375
- down_weight: bfloat16 [32, 2048, 4096], P('ep', None, 'tp'), may hold values from -0.125 to 0.125
Outputs:
- mixed_rows: bfloat16 [16384, 4096], P('ep', 'tp')
- expert_rows: bfloat16 [4096, 4096], P('ep', 'tp')
Inputs may be any that keep to these rules, and one draw needn't show every extreme that they name: `expert_index`: each row names 2 different experts. Within each aligned block of 128 rows (the rows of one index of ep) no expert is named by more than 16 rows, and one expert, the same in every block, is named by exactly 16 rows.
All inputs are finite; a program needn't handle non-finite values.
Results may differ from a plain program's by a relative error of at most 0.007.
Values may be sent and summed in bfloat16 or wider, within the bound.
No kernel may reach another device: no remote copies, remote signals or barrier semaphores. Data moves between devices by JAX's collectives and lax.ppermute only.
A program may use at most 64 MiB of HBM per device.

v0:
```python
import jax
import jax.numpy as jnp
from jax import lax
from jax.sharding import PartitionSpec as P

POOL = 2048
TOP = 2


window_reach = 15
norm_eps = 1e-06


def passed_along(value, axis, by):
    size = lax.axis_size(axis)
    pairs = [(i, i + by) for i in range(size) if 0 <= i + by < size]
    return lax.ppermute(value, axis, pairs)


def laid_out(parts, dim):
    lengths = list(parts.shape[1:])
    lengths[dim] *= parts.shape[0]
    return jnp.moveaxis(parts, 0, dim).reshape(lengths)


def copy_for_each(value, axis):
    size = lax.axis_size(axis)
    return lax.all_to_all(
        jnp.broadcast_to(value[None], (size, *value.shape)), axis, 0, 0, tiled=True
    )


def gathered_copies(value, axis, dim):
    return laid_out(copy_for_each(value, axis), dim)


def pool_minus_self(extended, first_pos, group_size, channel_base):
    length = extended.shape[0] - window_reach
    channels = extended.shape[1]
    channel = channel_base + jnp.arange(channels, dtype=jnp.int32)
    window = jnp.power(2, channel // group_size + 1).astype(jnp.int32)
    running = jnp.zeros((length, channels), jnp.float32)
    for lag_count in range(window_reach + 1):
        shifted = extended[window_reach - lag_count : window_reach - lag_count + length]
        running = running + jnp.where(lag_count < window[None, :], shifted, 0.0)
    position = first_pos + jnp.arange(length, dtype=jnp.int32)
    counts = jnp.minimum(position[:, None] + 1, window[None, :]).astype(jnp.float32)
    return (running / counts - extended[window_reach:]).astype(jnp.bfloat16)


def slot_targets(indices, experts, capacity):
    flattened = indices.reshape(-1)
    one_hot = (flattened[:, None] == jnp.arange(experts, dtype=jnp.int32)[None, :]).astype(
        jnp.int32
    )
    earlier = jnp.cumsum(one_hot, axis=0) - one_hot
    return flattened * capacity + jnp.sum(earlier * one_hot, axis=1)


def shards(
    mix_input,
    mix_weight,
    expert_input,
    expert_index,
    route_share,
    norm_gain,
    gate_weight,
    up_weight,
    down_weight,
):
    tokens_mix, channels = mix_input.shape
    trailing = mix_input[tokens_mix - window_reach :]
    previous = passed_along(trailing, "ep", 1)
    extended = jnp.concatenate([previous, mix_input], axis=0).astype(jnp.float32)
    pooled = pool_minus_self(
        extended, lax.axis_index("ep") * tokens_mix, POOL // 4, lax.axis_index("tp") * channels
    )
    mixed_rows = jnp.dot(
        lax.all_gather(pooled, "tp", axis=1, tiled=True),
        mix_weight,
        preferred_element_type=jnp.float32,
    ).astype(jnp.bfloat16)
    tokens_exp = expert_input.shape[0]
    local_experts = gate_weight.shape[0]
    experts = local_experts * lax.axis_size("ep")
    capacity = 2 * tokens_exp * TOP // experts
    model_width = norm_gain.shape[0]
    targets = slot_targets(expert_index, experts, capacity)
    sources = jnp.repeat(jnp.arange(tokens_exp, dtype=jnp.int32), TOP)
    table = jnp.full((experts * capacity,), tokens_exp, jnp.int32).at[targets].set(sources)
    feature_block = expert_input.shape[1]
    padded = jnp.concatenate([expert_input, jnp.zeros((1, feature_block), jnp.bfloat16)], axis=0)
    outgoing = padded[table].reshape(experts, capacity, feature_block)
    arrived = lax.all_to_all(outgoing, "ep", split_axis=0, concat_axis=1, tiled=True)
    portion = lax.all_gather(arrived, "tp", axis=2, tiled=True)
    scaled = (portion.astype(jnp.float32) * norm_gain).astype(jnp.bfloat16)
    gate_acts = jnp.einsum("erd,edh->erh", scaled, gate_weight, preferred_element_type=jnp.float32)
    up_acts = jnp.einsum("erd,edh->erh", scaled, up_weight, preferred_element_type=jnp.float32)
    squares = jnp.sum(jnp.square(portion.astype(jnp.float32)), axis=2)
    inverse = lax.rsqrt(squares / model_width + norm_eps)[:, :, None]
    hidden = (jax.nn.silu(gate_acts * inverse) * (up_acts * inverse)).astype(jnp.bfloat16)
    produced = jnp.einsum(
        "erh,ehc->erc",
        gathered_copies(hidden, "tp", 2),
        down_weight,
        preferred_element_type=jnp.float32,
    ).astype(jnp.bfloat16)
    returned = lax.all_to_all(produced, "ep", split_axis=1, concat_axis=0, tiled=True)
    returned = returned.reshape(experts * capacity, returned.shape[2])
    picked = returned[targets].astype(jnp.float32).reshape(tokens_exp, TOP, returned.shape[1])
    shares = route_share / jnp.sum(route_share, axis=1, keepdims=True)
    expert_rows = jnp.sum(picked * shares[:, :, None], axis=1).astype(jnp.bfloat16)
    return (mixed_rows, expert_rows)


def solution(mesh):
    placed = (
        P("ep", "tp"),
        P(None, "tp"),
        P("ep", "tp"),
        P("ep", None),
        P("ep", None),
        P(),
        P("ep", None, "tp"),
        P("ep", None, "tp"),
        P("ep", None, "tp"),
    )
    return jax.shard_map(
        shards,
        mesh=mesh,
        in_specs=placed,
        out_specs=(P("ep", "tp"), P("ep", "tp")),
        check_vma=False,
    )
```

profile of v0, /device:TPU:1, one launch (start us, length us, event | category | flops | bytes accessed | tf_op | source)
XLA Modules:
  0.0 190.6 jit_solution(15322384750593228259)
XLA Ops:
  7.2 0.8 broadcast_multiply_fusion
  8.1 0.8 copy.27
  9.0 0.1 eq.25
  9.2 0.1 mul.314
  9.4 0.6 reduce-window.6
  10.0 0.2 slice_reduce_fusion
  10.5 1.4 scatter_custom_fusion
  11.9 0.8 concatenate.7
  12.8 1.9 %gather_fusion = bf16[512,256]{1,0:T(8,128)(2,1)S(1)} fusion(bf16[129,256]{1,0:T(8,128)(2,1)S(1)} %concatenate.7, s32[1024]{0:T(1024)S(1)} %pad_clamp_fusion.1), kind=kCustom, calls=%fused_computation | custom fusion | bytes 526336 | tf_op jit(solution)/shard_map/gather | solution.py:93
  14.7 24.9 %all_to_all.26 = bf16[32,16,256]{2,1,0:T(8,128)(2,1)} all-to-all(bf16[32,16,256]{2,1,0:T(8,128)(2,1)S(1)} %bitcast.67), channel_id=1, replica_groups=mesh['ep'=32,'tp'=16] {'ep'}, dimensions={0} | all-to-all | bytes 524288 | tf_op jit(solution)/shard_map/all_to_all | solution.py:94
  39.7 0.7 slice.58
  40.4 2.1 %collective-permute-start = (bf16[15,128]{1,0:T(8,128)(2,1)S(1)}, bf16[15,128]{1,0:T(8,128)(2,1)S(1)}, u32[]{:S(2)}, u32[]{:S(2)}) collective-permute-start(bf16[15,128]{1,0:T(8,128)(2,1)S(1)} %slice.58), channel_id=1, source_target_pairs={{0,16},{16,32},{32,48},{48,64},{64,80},{80,96},{96,112},{112,128},... | collective-permute-start | bytes 11528 | tf_op jit(solution)/shard_map/ppermute | solution.py:17
  42.7 47.3 %all-gather.5.cloned.1.call-done = bf16[1,512,4096]{2,1,0:T(8,128)(2,1)} async-done(((bf16[1,512,256]{2,1,0:T(8,128)(2,1)}), bf16[1,512,4096]{2,1,0:T(8,128)(2,1)}) %all-gather.5.cloned.1.call-update) | async-done | bytes 4194320 | tf_op jit(solution)/shard_map/all_gather | solution.py:95
  90.0 3.2 %fusion.1 = f32[512]{0:T(512)S(1)} fusion(bf16[1,512,4096]{2,1,0:T(8,128)(2,1)} %all-gather.5.cloned.1.call-done), kind=kLoop, calls=%fused_computation.6 | loop fusion | flops 6290944 | bytes 4196352 | tf_op jit(solution)/shard_map/reduce_sum | solution.py:99
  93.3 0.2 copy-done.1
  93.4 1.3 fusion.8
  94.7 1.3 fusion.17
  96.1 1.5 broadcast_in_dim.167
  97.6 3.9 %all-to-all-start.1 = ((bf16[16,1,512,128]{2,3,1,0:T(8,128)(2,1)}), bf16[16,1,512,128]{2,3,1,0:T(8,128)(2,1)S(1)}, u32[]{:S(2)}, u32[]{:S(2)}) async-start(bf16[16,1,512,128]{2,3,1,0:T(8,128)(2,1)} %broadcast_in_dim.167), calls=%async_computation.1 | async-start | bytes 4194304 | tf_op jit(solution)/shard_map/all_to_all | solution.py:28
  101.7 1.2 fusion.40
  103.0 53.5 %all-to-all-done.1 = bf16[16,1,512,128]{2,3,1,0:T(8,128)(2,1)S(1)} async-done(((bf16[16,1,512,128]{2,3,1,0:T(8,128)(2,1)}), bf16[16,1,512,128]{2,3,1,0:T(8,128)(2,1)S(1)}, u32[]{:S(2)}, u32[]{:S(2)}) %all-to-all-start.1) | async-done | bytes 2097184 | tf_op jit(solution)/shard_map/all_to_all | solution.py:28
  156.4 0.8 fusion.7
  157.2 0.4 copy.40
  157.6 0.5 broadcast.1945
  158.1 2.3 %reduce.3 = bf16[512,256]{1,0:T(8,128)(2,1)S(1)} reduce(bf16[512,1,256]{2,1,0:T(2,128)(2,1)S(1)} %bitcast.65, bf16[]{:T(256)} %broadcast.1945), dimensions={1}, to_apply=%bitcast.60.reduce_sub_computation | reduce | bytes 524290
  160.4 0.8 reshape.278
  161.2 9.5 %all-to-all-start.2 = ((bf16[32,2,2048]{2,1,0:T(2,128)(2,1)}), bf16[32,2,2048]{2,1,0:T(2,128)(2,1)S(1)}, u32[]{:S(2)}, u32[]{:S(2)}) async-start(bf16[32,2,2048]{2,1,0:T(2,128)(2,1)} %reshape.278), calls=%async_computation.2 | async-start | bytes 524288 | tf_op jit(solution)/shard_map/all_to_all | solution.py:108
  170.9 3.3 %convolution_convert_fusion.1 = bf16[512,256]{1,0:T(8,128)(2,1)} fusion(bf16[512,2048]{1,0:T(8,128)(2,1)} %all-gather.3.cloned.1.call-done, bf16[2048,256]{1,0:T(8,128)(2,1)} %param.10), kind=kOutput, calls=%fused_computation.11 | convolution fusion | flops 537001984 | bytes 3407872 | tf_op jit(solution)/shard_map/dot_general | solution.py:78
  174.2 7.0 %all-to-all-done.2 = bf16[32,2,2048]{2,1,0:T(2,128)(2,1)S(1)} async-done(((bf16[32,2,2048]{2,1,0:T(2,128)(2,1)}), bf16[32,2,2048]{2,1,0:T(2,128)(2,1)S(1)}, u32[]{:S(2)}, u32[]{:S(2)}) %all-to-all-start.2) | async-done | bytes 262176 | tf_op jit(solution)/shard_map/all_to_all | solution.py:108
  181.1 0.3 reshape.279
  181.5 1.2 gather_fusion.1
  182.7 1.0 multiply_reduce_fusion
  (49 shorter events, 1.4 us)
Async XLA Ops:
  7.2 149.3 %copy-start = (bf16[1,2048,256]{2,1,0:T(8,128)(2,1)S(1)}, bf16[1,2048,256]{2,1,0:T(8,128)(2,1)}, u32[]{:S(2)}) copy-start(bf16[1,2048,256]{2,1,0:T(8,128)(2,1)} %param.17) | copy-start | bytes 3145732
  7.2 86.1 %copy-start.6 = (f32[4096]{0:T(1024)S(1)}, f32[4096]{0:T(1024)}, u32[]{:S(2)}) copy-start(f32[4096]{0:T(1024)} %param.14) | copy-start | bytes 49156
  7.2 86.1 %copy-start.4 = (bf16[1,4096,128]{2,1,0:T(8,128)(2,1)S(1)}, bf16[1,4096,128]{2,1,0:T(8,128)(2,1)}, u32[]{:S(2)}) copy-start(bf16[1,4096,128]{2,1,0:T(8,128)(2,1)} %param.15) | copy-start | bytes 3145732
  7.2 82.8 %all-gather.5.cloned.1.call-start = ((), (), s32[]{:S(2)}) async-start(), calls=%async_computation.4 | async-start | bytes 4456448 | tf_op jit(solution)/shard_map/all_gather | solution.py:95
  40.4 61.3 %collective-permute-start = (bf16[15,128]{1,0:T(8,128)(2,1)S(1)}, bf16[15,128]{1,0:T(8,128)(2,1)S(1)}, u32[]{:S(2)}, u32[]{:S(2)}) collective-permute-start(bf16[15,128]{1,0:T(8,128)(2,1)S(1)} %slice.58), channel_id=1, source_target_pairs={{0,16},{16,32},{32,48},{48,64},{64,80},{80,96},{96,112},{112,128},... | collective-permute-start | bytes 11528 | tf_op jit(solution)/shard_map/ppermute | solution.py:17
  90.0 3.4 %copy-start.1 = (bf16[1,512,4096]{2,1,0:T(8,128)(2,1)S(1)}, bf16[1,512,4096]{2,1,0:T(8,128)(2,1)}, u32[]{:S(2)}) copy-start(bf16[1,512,4096]{2,1,0:T(8,128)(2,1)} %all-gather.5.cloned.1.call-done) | copy-start | bytes 12582916
  93.2 1.5 copy-start.5
  96.0 5.7 %copy-start.2 = (bf16[512,128]{1,0:T(8,128)(2,1)S(1)}, bf16[512,128]{1,0:T(8,128)(2,1)}, u32[]{:S(2)}) copy-start(bf16[512,128]{1,0:T(8,128)(2,1)} %param.9) | copy-start | bytes 393220
  97.6 5.3 %copy-start.3 = (f32[128,2]{0,1:T(2,128)S(1)}, f32[128,2]{0,1:T(2,128)}, u32[]{:S(2)}) copy-start(f32[128,2]{0,1:T(2,128)} %param.13) | copy-start | bytes 3076
  97.6 58.8 %all-to-all-start.1 = ((bf16[16,1,512,128]{2,3,1,0:T(8,128)(2,1)}), bf16[16,1,512,128]{2,3,1,0:T(8,128)(2,1)S(1)}, u32[]{:S(2)}, u32[]{:S(2)}) async-start(bf16[16,1,512,128]{2,3,1,0:T(8,128)(2,1)} %broadcast_in_dim.167), calls=%async_computation.1 | async-start | bytes 4194304 | tf_op jit(solution)/shard_map/all_to_all | solution.py:28
  101.5 69.4 %all-gather.3.cloned.1.call-start = ((), (), s32[]{:S(2)}) async-start(), calls=%async_computation.3 | async-start | bytes 2228224 | tf_op jit(solution)/shard_map/all_gather | solution.py:79
  161.2 19.9 %all-to-all-start.2 = ((bf16[32,2,2048]{2,1,0:T(2,128)(2,1)}), bf16[32,2,2048]{2,1,0:T(2,128)(2,1)S(1)}, u32[]{:S(2)}, u32[]{:S(2)}) async-start(bf16[32,2,2048]{2,1,0:T(2,128)(2,1)} %reshape.278), calls=%async_computation.2 | async-start | bytes 524288 | tf_op jit(solution)/shard_map/all_to_all | solution.py:108
Sparse Core Ops, SparseCore 0:
  39.8 50.1 all-gather.4
  105.0 63.7 all-gather.2
where the time goes:
time: 192 us; the launch traced here: 191 us
  waiting for transfers between devices  108 us (56%)
  blocking collectives  24.9 us (13%)
  starting transfers between devices  15.6 us (8%)
  between operations  14.3 us (7%)
  local copies, waits for them, and re-layouts  11.8 us (6%)
  other arithmetic  9.6 us (5%)
  matrix products  6.55 us (3%)
    all_to_all x1, waiting for transfers between devices, copy_for_each(): lax.all_to_all(jnp.broadcast_to(value[None], (size, *value.shape)), axis,...  53.5 us
    all_gather x1, waiting for transfers between devices, shards(): portion = lax.all_gather(arrived, 'tp', axis=2, tiled=True)  47.3 us
    all_to_all x1, blocking collectives, shards(): lax.all_to_all(outgoing, 'ep', split_axis=0, concat_axis=1, tiled=True)  24.9 us
    all_to_all x1, starting transfers between devices, shards(): lax.all_to_all(produced, 'ep', split_axis=1, concat_axis=0, tiled=True)  9.53 us
    all_to_all x1, waiting for transfers between devices, shards(): lax.all_to_all(produced, 'ep', split_axis=1, concat_axis=0, tiled=True)  6.97 us
    all_to_all x1, starting transfers between devices, copy_for_each(): lax.all_to_all(jnp.broadcast_to(value[None], (size, *value.shape)), axis,...  3.91 us
  transfers between devices with their start and end apart: 5, of which 3 were waited for; matrix products, arithmetic and copies ran while one was open for 9% of the time, Pallas kernels for 0%

commit v1 on v0

v1 whole, which is shorter than its diff:
```python
import functools

import jax
import jax.numpy as jnp
from jax import lax
from jax.experimental import pallas as pl
from jax.experimental.pallas import tpu as pltpu
from jax.sharding import PartitionSpec as P

POOL = 2048
GROUPS = 4
TOP = 2
HALO = 16
norm_eps = 1e-06

VMEM = pl.BlockSpec(memory_space=pltpu.VMEM)
SMEM = pl.BlockSpec(memory_space=pltpu.SMEM)


def dot(a, b, dims=((1,), (0,))):
    return lax.dot_general(a, b, (dims, ((), ())), preferred_element_type=jnp.float32)


def slots_of(index, experts, capacity):
    tokens = index.shape[0]
    lanes = lax.broadcasted_iota(jnp.int32, (tokens, experts), 1)
    first, second = lanes == index[:, 0:1], lanes == index[:, 1:2]
    named = jnp.where(first | second, 1.0, 0.0)
    row = lax.broadcasted_iota(jnp.int32, (tokens, tokens), 0)
    col = lax.broadcasted_iota(jnp.int32, (tokens, tokens), 1)
    before = jnp.where(col < row, 1.0, 0.0).astype(jnp.bfloat16)
    earlier = dot(before, named.astype(jnp.bfloat16))
    slot = jnp.where(first | second, earlier, -1.0).astype(jnp.bfloat16)
    expert = lax.broadcasted_iota(jnp.int32, (experts, experts * capacity), 0)
    place = lax.broadcasted_iota(jnp.int32, (experts, experts * capacity), 1)
    spread = jnp.where(place // capacity == expert, 1.0, 0.0).astype(jnp.bfloat16)
    wanted = lax.broadcasted_iota(jnp.int32, (tokens, experts * capacity), 1) % capacity
    hit = dot(slot, spread) == wanted.astype(jnp.float32)
    return hit, first, second, spread


def dispatch_kernel(experts, capacity, index_ref, rows_ref, out_ref):
    hit, _, _, _ = slots_of(index_ref[...], experts, capacity)
    placed = jnp.where(hit, 1.0, 0.0).astype(jnp.bfloat16)
    out_ref[...] = dot(placed, rows_ref[...], ((0,), (0,))).astype(out_ref.dtype)


def dispatch(index, rows, experts, capacity):
    return pl.pallas_call(
        functools.partial(dispatch_kernel, experts, capacity),
        out_shape=jax.ShapeDtypeStruct((experts * capacity, rows.shape[1]), rows.dtype),
        in_specs=[VMEM, VMEM],
        out_specs=VMEM,
        name="dispatch",
        cost_estimate=pl.CostEstimate(flops=50_000_000, bytes_accessed=400_000, transcendentals=0),
    )(index, rows)


def shares_kernel(experts, capacity, index_ref, share_ref, high_ref, low_ref):
    hit, first, second, spread = slots_of(index_ref[...], experts, capacity)
    share = share_ref[...]
    share = share / (share[:, 0:1] + share[:, 1:2])
    by_expert = jnp.where(first, share[:, 0:1], jnp.where(second, share[:, 1:2], 0.0))
    high = by_expert.astype(jnp.bfloat16)
    low = (by_expert - high.astype(jnp.float32)).astype(jnp.bfloat16)
    high_ref[...] = jnp.where(hit, dot(high, spread), 0.0).astype(jnp.bfloat16)
    low_ref[...] = jnp.where(hit, dot(low, spread), 0.0).astype(jnp.bfloat16)


def weights_of_slots(index, share, experts, capacity):
    shape = jax.ShapeDtypeStruct((index.shape[0], experts * capacity), jnp.bfloat16)
    return pl.pallas_call(
        functools.partial(shares_kernel, experts, capacity),
        out_shape=(shape, shape),
        in_specs=[VMEM, VMEM],
        out_specs=(VMEM, VMEM),
        name="shares",
        cost_estimate=pl.CostEstimate(flops=20_000_000, bytes_accessed=300_000, transcendentals=0),
    )(index, share)


def combine_kernel(high_ref, low_ref, rows_ref, out_ref):
    rows = rows_ref[...]
    out_ref[...] = (dot(high_ref[...], rows) + dot(low_ref[...], rows)).astype(out_ref.dtype)


def combine(high, low, rows):
    return pl.pallas_call(
        combine_kernel,
        out_shape=jax.ShapeDtypeStruct((high.shape[0], rows.shape[1]), jnp.bfloat16),
        in_specs=[VMEM] * 3,
        out_specs=VMEM,
        name="combine",
        cost_estimate=pl.CostEstimate(flops=70_000_000, bytes_accessed=600_000, transcendentals=0),
    )(high, low, rows)


def pool_kernel(place_ref, before_ref, rows_ref, out_ref):
    rows = rows_ref[...].astype(jnp.float32)
    tokens = rows.shape[0]
    total = jnp.concatenate([before_ref[...].astype(jnp.float32), rows], axis=0)
    group = place_ref[1]
    window = 1
    picked = jnp.zeros_like(rows)
    for step in range(GROUPS):
        total = total + jnp.concatenate(
            [jnp.zeros((window, total.shape[1]), jnp.float32), total[:-window]], axis=0
        )
        window *= 2
        picked = jnp.where(group == step, total[HALO:], picked)
    position = place_ref[0] + lax.broadcasted_iota(jnp.int32, rows.shape, 0)
    width = jnp.left_shift(2, group)
    counts = jnp.minimum(position + 1, width).astype(jnp.float32)
    out_ref[...] = (picked / counts - rows).astype(out_ref.dtype)


def pool(place, before, rows):
    return pl.pallas_call(
        pool_kernel,
        out_shape=jax.ShapeDtypeStruct(rows.shape, rows.dtype),
        in_specs=[SMEM, VMEM, VMEM],
        out_specs=VMEM,
        name="pool",
        cost_estimate=pl.CostEstimate(flops=1_000_000, bytes_accessed=300_000, transcendentals=0),
    )(place, before, rows)


def hidden_kernel(blocks, width, rows_ref, gain_ref, gate_ref, up_ref, out_ref, gates, ups, squares):
    block = pl.program_id(0)
    rows = rows_ref[0].astype(jnp.float32)
    scaled = (rows * gain_ref[...]).astype(jnp.bfloat16)
    gate, up = dot(scaled, gate_ref[0]), dot(scaled, up_ref[0])
    square = jnp.square(rows)
    square = sum(square[:, at : at + 128] for at in range(0, rows.shape[1], 128))

    @pl.when(block == 0)
    def _():
        gates[...], ups[...], squares[...] = gate, up, square

    @pl.when(block > 0)
    def _():
        gates[...] += gate
        ups[...] += up
        squares[...] += square

    @pl.when(block == blocks - 1)
    def _():
        mean = jnp.sum(squares[...], axis=1, keepdims=True) / width
        inverse = lax.rsqrt(mean + norm_eps)
        gate_acts = gates[...] * inverse
        out_ref[...] = (gate_acts / (1.0 + jnp.exp(-gate_acts)) * (ups[...] * inverse)).astype(
            out_ref.dtype
        )


def hidden_of(gathered, gain, gate_weight, up_weight, features):
    blocks, rows, _ = gathered.shape
    hidden = gate_weight.shape[2]
    return pl.pallas_call(
        functools.partial(hidden_kernel, blocks, gain.shape[1]),
        out_shape=jax.ShapeDtypeStruct((rows, hidden), jnp.bfloat16),
        grid=(blocks,),
        in_specs=[
            pl.BlockSpec((1, rows, features), lambda k: (k, 0, 0)),
            pl.BlockSpec((1, features), lambda k: (0, k)),
            pl.BlockSpec((1, features, hidden), lambda k: (0, k, 0)),
            pl.BlockSpec((1, features, hidden), lambda k: (0, k, 0)),
        ],
        out_specs=pl.BlockSpec((rows, hidden), lambda k: (0, 0)),
        scratch_shapes=[
            pltpu.VMEM((rows, hidden), jnp.float32),
            pltpu.VMEM((rows, hidden), jnp.float32),
            pltpu.VMEM((rows, 128), jnp.float32),
        ],
        name="hidden",
        cost_estimate=pl.CostEstimate(
            flops=4 * rows * blocks * features * hidden, bytes_accessed=6_500_000, transcendentals=65536
        ),
    )(gathered, gain, gate_weight, up_weight)


def mix_kernel(blocks, rows_ref, weight_ref, out_ref, total):
    block = pl.program_id(0)
    part = dot(rows_ref[0], weight_ref[...])

    @pl.when(block == 0)
    def _():
        total[...] = part

    @pl.when(block > 0)
    def _():
        total[...] += part

    @pl.when(block == blocks - 1)
    def _():
        out_ref[...] = total[...].astype(out_ref.dtype)


def mixed_of(gathered, weight, first, channels):
    blocks, rows, _ = gathered.shape
    columns = weight.shape[1]
    return pl.pallas_call(
        functools.partial(mix_kernel, blocks),
        out_shape=jax.ShapeDtypeStruct((rows, columns), jnp.bfloat16),
        grid=(blocks,),
        in_specs=[
            pl.BlockSpec((1, rows, channels), lambda k: (k, 0, first // channels)),
            pl.BlockSpec((channels, columns), lambda k: (k, 0)),
        ],
        out_specs=pl.BlockSpec((rows, columns), lambda k: (0, 0)),
        scratch_shapes=[pltpu.VMEM((rows, columns), jnp.float32)],
        name="mixed",
        cost_estimate=pl.CostEstimate(
            flops=2 * rows * blocks * channels * columns, bytes_accessed=3_500_000, transcendentals=0
        ),
    )(gathered, weight)


def down_kernel(core_ref, own_ref, other_ref, own_weight_ref, other_weight_ref, out_ref, total):
    block = pl.program_id(0)
    part = dot(own_ref[0], own_weight_ref[0, 0]) + dot(other_ref[0], other_weight_ref[0, 0])

    @pl.when(block == 0)
    def _():
        total[...] = part

    @pl.when(block > 0)
    def _():
        total[...] += part

    @pl.when(block == pl.num_programs(0) - 1)
    def _():
        out_ref[...] = total[...].astype(out_ref.dtype)


def down(core, own, other, weight):
    blocks, rows, units = own.shape
    columns = weight.shape[3]
    return pl.pallas_call(
        down_kernel,
        grid_spec=pltpu.PrefetchScalarGridSpec(
            num_scalar_prefetch=1,
            grid=(blocks,),
            in_specs=[
                pl.BlockSpec((1, rows, units), lambda k, c: (k, 0, 0)),
                pl.BlockSpec((1, rows, units), lambda k, c: (k, 0, 0)),
                pl.BlockSpec((1, 1, units, columns), lambda k, c: (k, c[0], 0, 0)),
                pl.BlockSpec((1, 1, units, columns), lambda k, c: (k, 1 - c[0], 0, 0)),
            ],
            out_specs=pl.BlockSpec((rows, columns), lambda k, c: (0, 0)),
            scratch_shapes=[pltpu.VMEM((rows, columns), jnp.float32)],
        ),
        out_shape=jax.ShapeDtypeStruct((rows, columns), jnp.bfloat16),
        name="down",
        cost_estimate=pl.CostEstimate(
            flops=4 * rows * blocks * units * columns, bytes_accessed=3_500_000, transcendentals=0
        ),
    )(core, own, other, weight, weight)


def shards(
    mix_input,
    mix_weight,
    expert_input,
    expert_index,
    route_share,
    norm_gain,
    gate_weight,
    up_weight,
    down_weight,
):
    n_ep, n_tp = lax.axis_size("ep"), lax.axis_size("tp")
    chips = n_tp // 2
    ep, tp = lax.axis_index("ep"), lax.axis_index("tp")
    tokens_exp, features = expert_input.shape
    capacity = 2 * tokens_exp * TOP // n_ep

    outgoing = dispatch(expert_index, expert_input, n_ep, capacity)
    outgoing = outgoing.reshape(n_ep, capacity, features)
    arrived = lax.all_to_all(outgoing, "ep", 0, 0, tiled=True).reshape(n_ep * capacity, features)

    tokens_mix, channels = mix_input.shape
    before = lax.ppermute(
        mix_input[tokens_mix - HALO :], "ep", [(i, i + 1) for i in range(n_ep - 1)]
    )
    place = jnp.stack([ep * tokens_mix, tp * channels * GROUPS // POOL]).astype(jnp.int32)
    pooled = pool(place, before, mix_input)

    gathered = lax.all_gather(jnp.concatenate([arrived, pooled], axis=1), "tp", axis=0)
    hidden = hidden_of(gathered, norm_gain.reshape(1, -1), gate_weight, up_weight, features)
    mixed_rows = mixed_of(gathered, mix_weight, features, channels)

    columns_of_chips = [[chip * 2 + core for chip in range(chips)] for core in range(2)]
    partners = [(i, i + 1 - 2 * (i % 2)) for i in range(n_tp)]
    own = lax.all_to_all(
        jnp.broadcast_to(hidden[None], (chips, *hidden.shape)),
        "tp",
        0,
        0,
        tiled=True,
        axis_index_groups=columns_of_chips,
    )
    other = lax.ppermute(own, "tp", partners)
    core = (tp % 2).astype(jnp.int32).reshape(1)
    units = hidden.shape[1]
    produced = down(core, own, other, down_weight.reshape(chips, 2, units, down_weight.shape[2]))

    returned = lax.all_to_all(
        produced.reshape(n_ep, capacity, produced.shape[1]), "ep", 0, 0, tiled=True
    )
    high, low = weights_of_slots(expert_index, route_share, n_ep, capacity)
    expert_rows = combine(high, low, returned.reshape(n_ep * capacity, produced.shape[1]))
    return (mixed_rows, expert_rows)


def solution(mesh):
    placed = (
        P("ep", "tp"),
        P(None, "tp"),
        P("ep", "tp"),
        P("ep", None),
        P("ep", None),
        P(),
        P("ep", None, "tp"),
        P("ep", None, "tp"),
        P("ep", None, "tp"),
    )
    return jax.shard_map(
        shards,
        mesh=mesh,
        in_specs=placed,
        out_specs=(P("ep", "tp"), P("ep", "tp")),
        check_vma=False,
    )
```

time: 192 us -> 179 us (0.932)
  waiting for transfers between devices: 108 us -> 55.5 us
  Pallas kernels: 0 us -> 37.4 us
  starting transfers between devices: 15.6 us -> 29.8 us
  blocking collectives: 24.9 us -> 32.4 us
  other arithmetic: 9.6 us -> 2.36 us
  matrix products: 6.55 us -> 0 us
  local copies, waits for them, and re-layouts: 11.8 us -> 6.2 us
    all_to_all x2, waiting for transfers between devices: 60.4 us -> 4.33 us  [the longest x1 4.32 us: shards(): lax.all_to_all(outgoing, 'ep', 0, 0, tiled=True)]
    pallas_call x0 -> x7, Pallas kernels: none -> 37.4 us  [the longest x1 12.4 us: hidden_of(): pl.pallas_call(functools.partial(hidden_kernel, blocks, gain.shape[1]), o...]
    all_to_all x2, starting transfers between devices: 13.4 us -> 23.6 us  [the longest x1 13.7 us: shards(): lax.all_to_all(outgoing, 'ep', 0, 0, tiled=True)]
    all_to_all x1, blocking collectives: 24.9 us -> 32.4 us  [shards(): lax.all_to_all(jnp.broadcast_to(hidden[None], (chips, *hidden.shape)), 't...]
    dot_general x4 -> x0, matrix products: 6.55 us -> none  [the longest x1 3.27 us: shards(): jnp.dot(lax.all_gather(pooled, 'tp', axis=1, tiled=True), mix_weight, pre...]
    reduce_sum x4 -> x0, other arithmetic: 4.38 us -> none  [the longest x1 3.23 us: shards(): squares = jnp.sum(jnp.square(portion.astype(jnp.float32)), axis=2)]
    ppermute x1 -> x2, starting transfers between devices: 2.11 us -> 6.14 us  [the longest x1 3.12 us: shards(): lax.ppermute(mix_input[tokens_mix - HALO:], 'ep', [(i, i + 1) for i in ra...]
    gather x2 -> x0, local copies, waits for them, and re-layouts: 3.1 us -> none  [the longest x1 1.95 us: shards(): outgoing = padded[table].reshape(experts, capacity, feature_block)]
  transfers between devices with their start and end apart: 5 -> 5, of which waited for: 3 -> 4; matrix products, arithmetic and copies ran while one was open for 9% -> 1% of each run, Pallas kernels for 0% -> 8%
where the time goes in v1:
time: 179 us; the launch traced here: 178 us
  waiting for transfers between devices  55.5 us (31%)
  Pallas kernels  37.4 us (21%)
  blocking collectives  32.4 us (18%)
  starting transfers between devices  29.8 us (17%)
  between operations  14.1 us (8%)
  local copies, waits for them, and re-layouts  6.2 us (3%)
  other arithmetic  2.36 us (1%)
    all_gather x1, waiting for transfers between devices, shards(): lax.all_gather(jnp.concatenate([arrived, pooled], axis=1), 'tp', axis=0)  48.9 us
    all_to_all x1, blocking collectives, shards(): lax.all_to_all(jnp.broadcast_to(hidden[None], (chips, *hidden.shape)), 't...  32.4 us
    all_to_all x1, starting transfers between devices, shards(): lax.all_to_all(outgoing, 'ep', 0, 0, tiled=True)  13.7 us
    pallas_call x1, Pallas kernels, hidden_of(): pl.pallas_call(functools.partial(hidden_kernel, blocks, gain.shape[1]), o...  12.4 us
    pallas_call x1, Pallas kernels, mixed_of(): pl.pallas_call(functools.partial(mix_kernel, blocks), out_shape=jax.Shape...  10.6 us
    all_to_all x1, starting transfers between devices, shards(): lax.all_to_all(produced.reshape(n_ep, capacity, produced.shape[1]), 'ep',...  9.91 us
    pallas_call x1, Pallas kernels, down(): pl.pallas_call(down_kernel, grid_spec=pltpu.PrefetchScalarGridSpec(num_sc...  6.49 us
    unnamed x12, local copies, waits for them, and re-layouts  4.47 us
  transfers between devices with their start and end apart: 5, of which 4 were waited for; matrix products, arithmetic and copies ran while one was open for 1% of the time, Pallas kernels for 8%

profile of v1, /device:TPU:1, one launch (start us, length us, event | category | flops | bytes accessed | tf_op | source)
XLA Modules:
  0.0 177.9 jit_solution(11838407982249219757)
XLA Ops:
  7.2 1.4 copy.11.index_ref
  8.6 2.2 %dispatch.1 = bf16[512,256]{1,0:T(8,128)(2,1)} custom-call(s32[128,2]{1,0:T(8,128)} %copy.11.index_ref, bf16[128,256]{1,0:T(8,128)(2,1)} %rows_ref.2), custom_call_target="tpu_custom_call" | custom-call | flops 50000000 | bytes 400000 | tf_op jit(solution)/shard_map/dispatch/pallas_call | solution.py:49
  10.8 13.7 %all-to-all-start = ((bf16[32,16,256]{2,1,0:T(8,128)(2,1)}), bf16[32,16,256]{2,1,0:T(8,128)(2,1)S(1)}, u32[]{:S(2)}, u32[]{:S(2)}) async-start(bf16[32,16,256]{2,1,0:T(8,128)(2,1)} %bitcast.16), calls=%async_computation | async-start | bytes 524288 | tf_op jit(solution)/shard_map/all_to_all | solution.py:280
  24.5 0.0 all-gather.3.cloned.1.call-start
  24.6 0.7 slice.3
  25.3 3.1 %collective-permute-start = (bf16[16,128]{1,0:T(8,128)(2,1)S(1)}, bf16[16,128]{1,0:T(8,128)(2,1)S(1)}, u32[]{:S(2)}, u32[]{:S(2)}) collective-permute-start(bf16[16,128]{1,0:T(8,128)(2,1)S(1)} %slice.3), channel_id=1, source_target_pairs={{0,16},{16,32},{32,48},{48,64},{64,80},{80,96},{96,112},{112,128},... | collective-permute-start | bytes 12296 | tf_op jit(solution)/shard_map/ppermute | solution.py:283
  28.4 0.7 pad_add_fusion.place_ref
  29.1 0.1 collective-permute-done.before_ref
  29.1 0.0 copy-start.3
  29.1 0.6 copy-done.3
  29.7 1.8 %pool.1 = bf16[512,128]{1,0:T(8,128)(2,1)} custom-call(s32[2]{0:T(128)} %pad_add_fusion.place_ref, bf16[16,128]{1,0:T(8,128)(2,1)} %copy-done.3, bf16[512,128]{1,0:T(8,128)(2,1)} %rows_ref.3), custom_call_target="tpu_custom_call" | custom-call | flops 1000000 | bytes 300000 | tf_op jit(solution)/shard_map/pool/pallas_call | solution.py:118
  31.5 4.3 %all-to-all-done = bf16[32,16,256]{2,1,0:T(8,128)(2,1)S(1)} async-done(((bf16[32,16,256]{2,1,0:T(8,128)(2,1)}), bf16[32,16,256]{2,1,0:T(8,128)(2,1)S(1)}, u32[]{:S(2)}, u32[]{:S(2)}) %all-to-all-start) | async-done | bytes 262176 | tf_op jit(solution)/shard_map/all_to_all | solution.py:280
  35.8 1.7 pad_maximum_fusion
  37.5 0.0 all-gather.3.cloned.1.call-update
  37.6 48.9 %all-gather.3.cloned.1.call-done = bf16[8192,384]{1,0:T(8,128)(2,1)} async-done(((bf16[512,384]{1,0:T(8,128)(2,1)}), bf16[8192,384]{1,0:T(8,128)(2,1)}) %all-gather.3.cloned.1.call-update) | async-done | bytes 6291472 | tf_op jit(solution)/shard_map/all_gather | solution.py:289
  86.4 0.0 copy-start.4
  86.4 12.4 %hidden.1 = bf16[512,128]{1,0:T(8,128)(2,1)} custom-call(bf16[16,512,384]{2,1,0:T(8,128)(2,1)} %bitcast.10, f32[1,4096]{1,0:T(1,128)} %bitcast.18, bf16[1,4096,128]{2,1,0:T(8,128)(2,1)} %gate_ref.1, bf16[1,4096,128]{2,1,0:T(8,128)(2,1)} %up_ref.1), custom_call_target="tpu_custom_call" | custom-call | flops 1073741824 | bytes 6500000 | tf_op jit(solution)/shard_map/hidden/pallas_call | solution.py:159
  98.8 1.0 broadcast_in_dim.2
  99.9 32.4 %all_to_all.15.own_ref = bf16[8,512,128]{2,1,0:T(8,128)(2,1)S(1)} all-to-all(bf16[8,512,128]{2,1,0:T(8,128)(2,1)S(1)} %broadcast_in_dim.2), channel_id=1, replica_groups={{0,2,4,6,8,10,12,14},{1,3,5,7,9,11,13,15},{16,18,20,22,24,26,28,30},{17..., dimensions={0} | all-to-all | bytes 2097152 | tf_op jit(solution)/shard_map/all_to_all | solution.py:295
  132.3 3.0 %collective-permute-start.1 = (bf16[8,512,128]{2,1,0:T(8,128)(2,1)S(1)}, bf16[8,512,128]{2,1,0:T(8,128)(2,1)S(1)}, u32[]{:S(2)}, u32[]{:S(2)}) collective-permute-start(bf16[8,512,128]{2,1,0:T(8,128)(2,1)S(1)} %all_to_all.15.own_ref), channel_id=1, source_target_pairs={{0,1},{1,0},{2,3},{3,2},{4,5},{5,4},{6,7},{7,6},{8,9},{9,8},{10,11... | collective-permute-start | bytes 3145736 | tf_op jit(solution)/shard_map/ppermute | solution.py:303
  135.3 2.3 %collective-permute-done.1.other_ref = bf16[8,512,128]{2,1,0:T(8,128)(2,1)S(1)} collective-permute-done((bf16[8,512,128]{2,1,0:T(8,128)(2,1)S(1)}, bf16[8,512,128]{2,1,0:T(8,128)(2,1)S(1)}, u32[]{:S(2)}, u32[]{:S(2)}) %collective-permute-start.1) | collective-permute-done | bytes 1048608 | tf_op jit(solution)/shard_map/ppermute | solution.py:303
  137.6 0.0 copy-done
  137.6 1.0 copy-done.1
  138.6 6.5 %down.1 = bf16[512,256]{1,0:T(8,128)(2,1)} custom-call(s32[1]{0:T(128)} %bitcast.5.core_ref, bf16[8,512,128]{2,1,0:T(8,128)(2,1)} %copy-done, bf16[8,512,128]{2,1,0:T(8,128)(2,1)} %copy-done.1, bf16[8,2,128,256]{3,2,1,0:T(8,128)(2,1)} %bitcast.12, bf16[8,2,128,256]{3,2,1,0:T(8,128)(2,1)} %bitcast.13), custom_call_target="tpu_custom_call" | custom-call | flops 536870912 | bytes 3500000 | tf_op jit(solution)/shard_map/down/pallas_call | solution.py:239
  145.1 9.9 %all-to-all-start.2 = ((bf16[32,16,256]{2,1,0:T(8,128)(2,1)}), bf16[32,16,256]{2,1,0:T(8,128)(2,1)S(1)}, u32[]{:S(2)}, u32[]{:S(2)}) async-start(bf16[32,16,256]{2,1,0:T(8,128)(2,1)} %bitcast.15), calls=%async_computation.2 | async-start | bytes 524288 | tf_op jit(solution)/shard_map/all_to_all | solution.py:308
  155.0 0.0 copy-done.4
  155.0 0.7 copy.13.share_ref
  155.8 2.0 %shares.1 = (bf16[128,512]{1,0:T(8,128)(2,1)}, bf16[128,512]{1,0:T(8,128)(2,1)}) custom-call(s32[128,2]{1,0:T(8,128)} %copy.11.index_ref, f32[128,2]{1,0:T(8,128)} %copy.13.share_ref), custom_call_target="tpu_custom_call" | custom-call | flops 20000000 | bytes 300000 | tf_op jit(solution)/shard_map/shares/pallas_call | solution.py:72
  157.8 10.6 %mixed.1 = bf16[512,256]{1,0:T(8,128)(2,1)} custom-call(bf16[16,512,384]{2,1,0:T(8,128)(2,1)} %bitcast.11, bf16[2048,256]{1,0:T(8,128)(2,1)} %weight_ref.1), custom_call_target="tpu_custom_call" | custom-call | flops 536870912 | bytes 3500000 | tf_op jit(solution)/shard_map/mixed/pallas_call | solution.py:202
  168.4 0.0 all-to-all-done.2
  168.4 0.7 copy-done.2
  169.1 1.9 %combine.1 = bf16[128,256]{1,0:T(8,128)(2,1)} custom-call(bf16[128,512]{1,0:T(8,128)(2,1)} %get-tuple-element.4.high_ref, bf16[128,512]{1,0:T(8,128)(2,1)} %get-tuple-element.5.low_ref, bf16[512,256]{1,0:T(8,128)(2,1)} %bitcast.17), custom_call_target="tpu_custom_call" | custom-call | flops 70000000 | bytes 600000 | tf_op jit(solution)/shard_map/combine/pallas_call | solution.py:88
  (3 shorter events, 0.0 us)
Async XLA Ops:
  10.8 25.0 %all-to-all-start = ((bf16[32,16,256]{2,1,0:T(8,128)(2,1)}), bf16[32,16,256]{2,1,0:T(8,128)(2,1)S(1)}, u32[]{:S(2)}, u32[]{:S(2)}) async-start(bf16[32,16,256]{2,1,0:T(8,128)(2,1)} %bitcast.16), calls=%async_computation | async-start | bytes 524288 | tf_op jit(solution)/shard_map/all_to_all | solution.py:280
  24.5 61.9 %all-gather.3.cloned.1.call-start = ((), (), s32[]{:S(2)}) async-start(), calls=%async_computation.3 | async-start | bytes 6684672 | tf_op jit(solution)/shard_map/all_gather | solution.py:289
  25.3 3.9 %collective-permute-start = (bf16[16,128]{1,0:T(8,128)(2,1)S(1)}, bf16[16,128]{1,0:T(8,128)(2,1)S(1)}, u32[]{:S(2)}, u32[]{:S(2)}) collective-permute-start(bf16[16,128]{1,0:T(8,128)(2,1)S(1)} %slice.3), channel_id=1, source_target_pairs={{0,16},{16,32},{32,48},{48,64},{64,80},{80,96},{96,112},{112,128},... | collective-permute-start | bytes 12296 | tf_op jit(solution)/shard_map/ppermute | solution.py:283
  29.1 0.6 copy-start.3
  86.4 68.6 %copy-start.4 = (f32[128,2]{0,1:T(2,128)S(1)}, f32[128,2]{0,1:T(2,128)}, u32[]{:S(2)}) copy-start(f32[128,2]{0,1:T(2,128)} %param.13) | copy-start | bytes 3076
  132.3 5.3 %copy-start = (bf16[8,512,128]{2,1,0:T(8,128)(2,1)}, bf16[8,512,128]{2,1,0:T(8,128)(2,1)S(1)}, u32[]{:S(2)}) copy-start(bf16[8,512,128]{2,1,0:T(8,128)(2,1)S(1)} %all_to_all.15.own_ref) | copy-start | bytes 3145732
  132.3 5.3 %collective-permute-start.1 = (bf16[8,512,128]{2,1,0:T(8,128)(2,1)S(1)}, bf16[8,512,128]{2,1,0:T(8,128)(2,1)S(1)}, u32[]{:S(2)}, u32[]{:S(2)}) collective-permute-start(bf16[8,512,128]{2,1,0:T(8,128)(2,1)S(1)} %all_to_all.15.own_ref), channel_id=1, source_target_pairs={{0,1},{1,0},{2,3},{3,2},{4,5},{5,4},{6,7},{7,6},{8,9},{9,8},{10,11... | collective-permute-start | bytes 3145736 | tf_op jit(solution)/shard_map/ppermute | solution.py:303
  137.6 1.0 copy-start.1
  145.1 23.3 %all-to-all-start.2 = ((bf16[32,16,256]{2,1,0:T(8,128)(2,1)}), bf16[32,16,256]{2,1,0:T(8,128)(2,1)S(1)}, u32[]{:S(2)}, u32[]{:S(2)}) async-start(bf16[32,16,256]{2,1,0:T(8,128)(2,1)} %bitcast.15), calls=%async_computation.2 | async-start | bytes 524288 | tf_op jit(solution)/shard_map/all_to_all | solution.py:308
  168.4 0.7 copy-start.2
Sparse Core Ops, SparseCore 0:
  37.7 48.7 all-gather.2

commit v2 on v1

v2 whole, which is shorter than its diff:
```python
import functools

import jax
import jax.numpy as jnp
from jax import lax
from jax.experimental import pallas as pl
from jax.experimental.pallas import tpu as pltpu
from jax.sharding import PartitionSpec as P

POOL = 2048
GROUPS = 4
TOP = 2
HALO = 16
norm_eps = 1e-06

VMEM = pl.BlockSpec(memory_space=pltpu.VMEM)
SMEM = pl.BlockSpec(memory_space=pltpu.SMEM)
HBM = pl.BlockSpec(memory_space=pltpu.HBM)
EARLY = 112


def room(mib):
    return pltpu.CompilerParams(vmem_limit_bytes=mib * 2**20)


def cost(flops, moved):
    return pl.CostEstimate(flops=flops, bytes_accessed=moved, transcendentals=0)


def dot(a, b, dims=((1,), (0,))):
    return lax.dot_general(a, b, (dims, ((), ())), preferred_element_type=jnp.float32)


def slots_of(index, experts, capacity):
    tokens = index.shape[1]
    expert = lax.broadcasted_iota(jnp.int32, (experts, tokens), 0)
    first, second = expert == index[0:1], expert == index[1:2]
    named = jnp.where(first | second, 1.0, 0.0).astype(jnp.bfloat16)
    row = lax.broadcasted_iota(jnp.int32, (tokens, tokens), 0)
    col = lax.broadcasted_iota(jnp.int32, (tokens, tokens), 1)
    before = jnp.where(row < col, 1.0, 0.0).astype(jnp.bfloat16)
    slot = jnp.where(first | second, dot(named, before), -1.0).astype(jnp.bfloat16)
    place = lax.broadcasted_iota(jnp.int32, (experts * capacity, experts), 0)
    lane = lax.broadcasted_iota(jnp.int32, (experts * capacity, experts), 1)
    spread = jnp.where(place // capacity == lane, 1.0, 0.0).astype(jnp.bfloat16)
    wanted = lax.broadcasted_iota(jnp.int32, (experts * capacity, tokens), 0) % capacity
    hit = dot(spread, slot) == wanted.astype(jnp.float32)
    return hit, first, second, spread


def dispatch_kernel(experts, capacity, index_ref, rows_ref, out_ref):
    hit, _, _, _ = slots_of(index_ref[...], experts, capacity)
    placed = jnp.where(hit, 1.0, 0.0).astype(jnp.bfloat16)
    out_ref[...] = dot(placed, rows_ref[...]).astype(out_ref.dtype)


def dispatch(index, rows, experts, capacity):
    return pl.pallas_call(
        functools.partial(dispatch_kernel, experts, capacity),
        out_shape=jax.ShapeDtypeStruct((experts * capacity, rows.shape[1]), rows.dtype),
        in_specs=[VMEM, VMEM],
        out_specs=VMEM,
        name="dispatch",
        compiler_params=room(8),
        cost_estimate=cost(50_000_000, 400_000),
    )(index, rows)


def shares_kernel(experts, capacity, index_ref, share_ref, high_ref, low_ref):
    hit, first, second, spread = slots_of(index_ref[...], experts, capacity)
    share = share_ref[...]
    share = share / (share[0:1] + share[1:2])
    by_expert = jnp.where(first, share[0:1], jnp.where(second, share[1:2], 0.0))
    high = by_expert.astype(jnp.bfloat16)
    low = (by_expert - high.astype(jnp.float32)).astype(jnp.bfloat16)
    high_ref[...] = jnp.where(hit, dot(spread, high), 0.0).T.astype(jnp.bfloat16)
    low_ref[...] = jnp.where(hit, dot(spread, low), 0.0).T.astype(jnp.bfloat16)


def weights_of_slots(index, share, experts, capacity):
    shape = jax.ShapeDtypeStruct((index.shape[1], experts * capacity), jnp.bfloat16)
    return pl.pallas_call(
        functools.partial(shares_kernel, experts, capacity),
        out_shape=(shape, shape),
        in_specs=[VMEM, VMEM],
        out_specs=(VMEM, VMEM),
        name="shares",
        compiler_params=room(8),
        cost_estimate=cost(20_000_000, 300_000),
    )(index, share)


def combine_kernel(high_ref, low_ref, rows_ref, out_ref):
    rows = rows_ref[...]
    out_ref[...] = (dot(high_ref[...], rows) + dot(low_ref[...], rows)).astype(out_ref.dtype)


def combine(high, low, rows):
    return pl.pallas_call(
        combine_kernel,
        out_shape=jax.ShapeDtypeStruct((high.shape[0], rows.shape[1]), jnp.bfloat16),
        in_specs=[VMEM] * 3,
        out_specs=VMEM,
        name="combine",
        compiler_params=room(8),
        cost_estimate=cost(70_000_000, 600_000),
    )(high, low, rows)


def pool_kernel(place_ref, before_ref, rows_ref, out_ref):
    rows = rows_ref[...].astype(jnp.float32)
    total = jnp.concatenate([before_ref[...].astype(jnp.float32), rows], axis=0)
    group = place_ref[1]
    window = 1
    picked = jnp.zeros_like(rows)
    for step in range(GROUPS):
        total = total + jnp.concatenate(
            [jnp.zeros((window, total.shape[1]), jnp.float32), total[:-window]], axis=0
        )
        window *= 2
        picked = jnp.where(group == step, total[HALO:], picked)
    position = place_ref[0] + lax.broadcasted_iota(jnp.int32, rows.shape, 0)
    width = jnp.left_shift(2, group)
    counts = jnp.minimum(position + 1, width).astype(jnp.float32)
    out_ref[...] = (picked / counts - rows).astype(out_ref.dtype)


def pool(place, before, rows):
    return pl.pallas_call(
        pool_kernel,
        out_shape=jax.ShapeDtypeStruct(rows.shape, rows.dtype),
        in_specs=[SMEM, VMEM, VMEM],
        out_specs=VMEM,
        name="pool",
        compiler_params=room(8),
        cost_estimate=cost(1_000_000, 300_000),
    )(place, before, rows)


def side_by_side(blocks):
    return jnp.concatenate([blocks[i] for i in range(blocks.shape[0])], axis=1)


def finish(total, squares, width):
    units = total.shape[1] // 2
    inverse = lax.rsqrt(jnp.sum(squares, axis=1, keepdims=True) / width + norm_eps)
    gates, ups = total[:, :units] * inverse, total[:, units:] * inverse
    return (gates / (1.0 + jnp.exp(-gates)) * ups).astype(jnp.bfloat16)


def products(rows, gain, gate, up):
    rows = rows.astype(jnp.float32)
    scaled = (rows * gain).astype(jnp.bfloat16)
    square = jnp.square(rows)
    square = sum(square[:, at : at + 128] for at in range(0, rows.shape[1], 128))
    return dot(scaled, jnp.concatenate([gate, up], axis=1)), square


def early_kernel(rows_ref, gain_ref, gate_ref, up_ref, out_ref):
    total, square = products(side_by_side(rows_ref), gain_ref[...], gate_ref[0], up_ref[0])
    out_ref[...] = finish(total, square, gain_ref.shape[1])


def early_hidden_of(gathered, gain, gate_weight, up_weight):
    blocks, rows, features = gathered.shape
    units = gate_weight.shape[2]
    return pl.pallas_call(
        early_kernel,
        out_shape=jax.ShapeDtypeStruct((rows, units), jnp.bfloat16),
        in_specs=[VMEM] * 4,
        out_specs=VMEM,
        name="early_hidden",
        compiler_params=room(24),
        cost_estimate=cost(4 * rows * blocks * features * units, 3_500_000),
    )(gathered, gain, gate_weight, up_weight)


def fetch(source_ref, first, held, sems):
    copies = []
    for block in range(held.shape[0]):
        piece = source_ref.at[block, pl.ds(first, held.shape[1])]
        copies.append(pltpu.make_async_copy(piece, held.at[block], sems.at[block]))
        copies[-1].start()
    return copies


def hidden_kernel(
    at_once, from_ref, gain_ref, gate_from, up_from, out_ref, held, gate_ref, up_ref, sems, sides
):
    weights = [
        pltpu.make_async_copy(gate_from, gate_ref, sides.at[0]),
        pltpu.make_async_copy(up_from, up_ref, sides.at[1]),
    ]
    for weight in weights:
        weight.start()
    copies = fetch(from_ref, 0, held, sems)
    for weight in weights:
        weight.wait()
    rows = out_ref.shape[1]
    pieces = held.shape[1] // rows
    depth = at_once * pieces * held.shape[2]
    total = square = 0.0
    for step in range(len(copies) // at_once):
        parts = []
        for block in range(step * at_once, (step + 1) * at_once):
            copies[block].wait()
            parts += [held[block, i * rows : (i + 1) * rows] for i in range(pieces)]
        part = slice(step * depth, (step + 1) * depth)
        more, squares = products(
            jnp.concatenate(parts, axis=1), gain_ref[:, part], gate_ref[0, part], up_ref[0, part]
        )
        total, square = total + more, square + squares
    hidden = finish(total, square, gain_ref.shape[1])
    for copy in range(out_ref.shape[0]):
        out_ref[copy] = hidden


def hidden_of(gathered, gain, gate_weight, up_weight, rows, pieces, copies):
    blocks, _, lanes = gathered.shape
    units = gate_weight.shape[2]
    return pl.pallas_call(
        functools.partial(hidden_kernel, 4),
        out_shape=jax.ShapeDtypeStruct((copies, rows, units), jnp.bfloat16),
        in_specs=[HBM, VMEM, HBM, HBM],
        out_specs=VMEM,
        scratch_shapes=[
            pltpu.VMEM((blocks, pieces * rows, lanes), jnp.bfloat16),
            pltpu.VMEM(gate_weight.shape, jnp.bfloat16),
            pltpu.VMEM(up_weight.shape, jnp.bfloat16),
            pltpu.SemaphoreType.DMA((blocks,)),
            pltpu.SemaphoreType.DMA((2,)),
        ],
        name="hidden",
        compiler_params=room(60),
        cost_estimate=cost(4 * rows * gain.shape[1] * units, 6_500_000),
    )(gathered, gain, gate_weight, up_weight)


def mix_kernel(at_once, first, from_ref, weight_ref, out_ref, held, sems):
    copies = fetch(from_ref, first, held, sems)
    depth = at_once * held.shape[2]
    total = 0.0
    for step in range(len(copies) // at_once):
        parts = []
        for block in range(step * at_once, (step + 1) * at_once):
            copies[block].wait()
            parts.append(held[block])
        part = weight_ref[step * depth : (step + 1) * depth]
        total = total + dot(jnp.concatenate(parts, axis=1), part)
    out_ref[...] = total.astype(out_ref.dtype)


def mixed_of(gathered, weight, first, rows):
    blocks, _, lanes = gathered.shape
    columns = weight.shape[1]
    return pl.pallas_call(
        functools.partial(mix_kernel, 4, first),
        out_shape=jax.ShapeDtypeStruct((rows, columns), jnp.bfloat16),
        in_specs=[HBM, VMEM],
        out_specs=VMEM,
        scratch_shapes=[
            pltpu.VMEM((blocks, rows, lanes), jnp.bfloat16),
            pltpu.SemaphoreType.DMA((blocks,)),
        ],
        name="mixed",
        compiler_params=room(60),
        cost_estimate=cost(2 * rows * blocks * lanes * columns, 3_500_000),
    )(gathered, weight)


def down_kernel(core_ref, early_ref, own_ref, other_ref, weight_ref, out_ref):
    core = core_ref[0]
    chips = own_ref.shape[0]
    units = early_ref.shape[2]
    split = early_ref.shape[1]
    weight = weight_ref[...].reshape(2 * chips * units, weight_ref.shape[2])
    out_ref[:split] = dot(side_by_side(early_ref), weight).astype(out_ref.dtype)
    mine = jnp.concatenate([weight_ref[2 * i + core] for i in range(chips)], axis=0)
    total = dot(side_by_side(own_ref), mine)
    theirs = jnp.concatenate([weight_ref[2 * i + 1 - core] for i in range(chips)], axis=0)
    out_ref[split:] = (total + dot(side_by_side(other_ref), theirs)).astype(out_ref.dtype)


def down(core, early, own, other, weight):
    columns = weight.shape[2]
    rows = early.shape[1] + own.shape[1]
    return pl.pallas_call(
        down_kernel,
        in_specs=[SMEM, VMEM, VMEM, VMEM, VMEM],
        out_specs=VMEM,
        out_shape=jax.ShapeDtypeStruct((rows, columns), jnp.bfloat16),
        name="down",
        compiler_params=room(16),
        cost_estimate=cost(2 * rows * weight.shape[0] * weight.shape[1] * columns, 3_500_000),
    )(core, early, own, other, weight)


def shards(
    mix_input,
    mix_weight,
    expert_input,
    expert_index,
    route_share,
    norm_gain,
    gate_weight,
    up_weight,
    down_weight,
):
    n_ep, n_tp = lax.axis_size("ep"), lax.axis_size("tp")
    chips = n_tp // 2
    ep, tp = lax.axis_index("ep"), lax.axis_index("tp")
    tokens_exp, features = expert_input.shape
    capacity = 2 * tokens_exp * TOP // n_ep
    units = gate_weight.shape[2]
    index, share, gain = expert_index.T, route_share.T, norm_gain.reshape(1, -1)

    outgoing = dispatch(index, expert_input, n_ep, capacity)
    outgoing = outgoing.reshape(n_ep, capacity, features)
    arrived = lax.all_to_all(outgoing, "ep", 0, 0, tiled=True).reshape(n_ep * capacity, features)

    tokens_mix, channels = mix_input.shape
    before = lax.ppermute(
        mix_input[tokens_mix - HALO :], "ep", [(i, i + 1) for i in range(n_ep - 1)]
    )
    place = jnp.stack([ep * tokens_mix, tp // (POOL // GROUPS // channels)]).astype(jnp.int32)
    pooled = pool(place, before, mix_input)

    late_rows = n_ep * capacity - EARLY
    pieces = features // channels
    sent = [arrived[EARLY:, i * channels : (i + 1) * channels] for i in range(pieces)]
    gathered = lax.all_gather(jnp.concatenate(sent + [pooled], axis=0), "tp", axis=0)
    early = lax.all_gather(arrived[:EARLY], "tp", axis=0)
    early_hidden = early_hidden_of(early, gain, gate_weight, up_weight)
    early_hidden = lax.all_gather(early_hidden, "tp", axis=0)
    gathered, early_hidden = lax.optimization_barrier((gathered, early_hidden))
    hidden = hidden_of(gathered, gain, gate_weight, up_weight, late_rows, pieces, chips)
    mixed_rows = mixed_of(gathered, mix_weight, pieces * late_rows, tokens_mix)

    columns_of_chips = [[chip * 2 + core for chip in range(chips)] for core in range(2)]
    partners = [(i, i + 1 - 2 * (i % 2)) for i in range(n_tp)]
    own = lax.all_to_all(hidden, "tp", 0, 0, tiled=True, axis_index_groups=columns_of_chips)
    other = lax.ppermute(own, "tp", partners)
    core = lax.rem(tp, 2).astype(jnp.int32).reshape(1)
    produced = down(
        core, early_hidden, own, other, down_weight.reshape(n_tp, units, down_weight.shape[2])
    )

    returned = lax.all_to_all(
        produced.reshape(n_ep, capacity, produced.shape[1]), "ep", 0, 0, tiled=True
    )
    high, low = weights_of_slots(index, share, n_ep, capacity)
    expert_rows = combine(high, low, returned.reshape(n_ep * capacity, produced.shape[1]))
    return (mixed_rows, expert_rows)


def solution(mesh):
    placed = (
        P("ep", "tp"),
        P(None, "tp"),
        P("ep", "tp"),
        P("ep", None),
        P("ep", None),
        P(),
        P("ep", None, "tp"),
        P("ep", None, "tp"),
        P("ep", None, "tp"),
    )
    return jax.shard_map(
        shards,
        mesh=mesh,
        in_specs=placed,
        out_specs=(P("ep", "tp"), P("ep", "tp")),
        check_vma=False,
    )
```

time: 179 us -> 154 us (0.86)
  waiting for transfers between devices: 55.5 us -> 14.8 us
  blocking collectives: 32.4 us -> 71.6 us
  Pallas kernels: 37.4 us -> 17.1 us
    all_gather x1, waiting for transfers between devices: 48.9 us -> 0.97 us  [shards(): lax.all_gather(jnp.concatenate(sent + [pooled], axis=0), 'tp', axis=0)]
    all_gather x0 -> x2, blocking collectives: none -> 43.9 us  [the longest x1 24.8 us: shards(): early = lax.all_gather(arrived[:EARLY], 'tp', axis=0)]
    pallas_call x3 -> x4, Pallas kernels: 29.5 us -> 13.8 us  [the longest x1 6.97 us: hidden_of(): pl.pallas_call(functools.partial(hidden_kernel, 4), out_shape=jax.ShapeDt...]
    all_to_all x1, waiting for transfers between devices: 0.01 us -> 6.2 us  [shards(): lax.all_to_all(produced.reshape(n_ep, capacity, produced.shape[1]), 'ep',...]
    all_to_all x1, blocking collectives: 32.4 us -> 27.8 us  [shards(): lax.all_to_all(hidden, 'tp', 0, 0, tiled=True, axis_index_groups=columns_...]
    unnamed x12 -> x18, local copies, waits for them, and re-layouts: 4.47 us -> 5.65 us
  transfers between devices with their start and end apart: 5 -> 5, of which waited for: 4 -> 5; matrix products, arithmetic and copies ran while one was open for 1% -> 1% of each run, Pallas kernels for 8% -> 4%
where the time goes in v2:
time: 154 us; the launch traced here: 153 us
  blocking collectives  71.6 us (46%)
  starting transfers between devices  28.3 us (18%)
  Pallas kernels  17.1 us (11%)
  waiting for transfers between devices  14.8 us (10%)
  between operations  14.2 us (9%)
  local copies, waits for them, and re-layouts  6.36 us (4%)
    all_to_all x1, blocking collectives, shards(): lax.all_to_all(hidden, 'tp', 0, 0, tiled=True, axis_index_groups=columns_...  27.8 us
    all_gather x1, blocking collectives, shards(): early = lax.all_gather(arrived[:EARLY], 'tp', axis=0)  24.8 us
    all_gather x1, blocking collectives, shards(): early_hidden = lax.all_gather(early_hidden, 'tp', axis=0)  19.1 us
    all_to_all x1, starting transfers between devices, shards(): lax.all_to_all(outgoing, 'ep', 0, 0, tiled=True)  13.7 us
    all_to_all x1, starting transfers between devices, shards(): lax.all_to_all(produced.reshape(n_ep, capacity, produced.shape[1]), 'ep',...  8.76 us
    pallas_call x1, Pallas kernels, hidden_of(): pl.pallas_call(functools.partial(hidden_kernel, 4), out_shape=jax.ShapeDt...  6.97 us
    all_to_all x1, waiting for transfers between devices, shards(): lax.all_to_all(produced.reshape(n_ep, capacity, produced.shape[1]), 'ep',...  6.2 us
    unnamed x18, local copies, waits for them, and re-layouts  5.65 us
  transfers between devices with their start and end apart: 5, of which 5 were waited for; matrix products, arithmetic and copies ran while one was open for 1% of the time, Pallas kernels for 4%

profile of v2, /device:TPU:1, one launch (start us, length us, event | category | flops | bytes accessed | tf_op | source)
XLA Modules:
  0.0 153.1 jit_solution(15768119091153803096)
XLA Ops:
  7.2 0.8 copy-done.5
  8.0 0.7 copy-done.6
  8.7 1.2 dispatch.1
  9.9 13.7 %all-to-all-start = ((bf16[32,16,256]{2,1,0:T(8,128)(2,1)}), bf16[32,16,256]{2,1,0:T(8,128)(2,1)S(1)}, u32[]{:S(2)}, u32[]{:S(2)}) async-start(bf16[32,16,256]{2,1,0:T(8,128)(2,1)} %bitcast.1), calls=%async_computation | async-start | bytes 524288 | tf_op jit(solution)/shard_map/all_to_all | solution.py:319
  23.6 0.0 all-gather.4.cloned.1.call-start
  23.6 0.7 slice.15
  24.3 3.1 %collective-permute-start = (bf16[16,128]{1,0:T(8,128)(2,1)S(1)}, bf16[16,128]{1,0:T(8,128)(2,1)S(1)}, u32[]{:S(2)}, u32[]{:S(2)}) collective-permute-start(bf16[16,128]{1,0:T(8,128)(2,1)S(1)} %slice.15), channel_id=1, source_target_pairs={{0,16},{16,32},{32,48},{48,64},{64,80},{80,96},{96,112},{112,128},... | collective-permute-start | bytes 12296 | tf_op jit(solution)/shard_map/ppermute | solution.py:322
  27.4 0.1 pad_add_fusion.place_ref
  27.5 0.6 collective-permute-done.before_ref
  28.2 0.9 copy-done.3
  29.1 0.8 pool.1
  29.8 5.0 %all-to-all-done = bf16[32,16,256]{2,1,0:T(8,128)(2,1)S(1)} async-done(((bf16[32,16,256]{2,1,0:T(8,128)(2,1)}), bf16[32,16,256]{2,1,0:T(8,128)(2,1)S(1)}, u32[]{:S(2)}, u32[]{:S(2)}) %all-to-all-start) | async-done | bytes 262176 | tf_op jit(solution)/shard_map/all_to_all | solution.py:319
  34.9 0.8 pad_maximum_fusion
  35.6 0.0 all-gather.4.cloned.1.call-update
  35.7 24.8 %all_gather.21.rows_ref = bf16[16,112,256]{2,1,0:T(8,128)(2,1)S(1)} all-gather(bf16[1,112,256]{2,1,0:T(8,128)(2,1)S(1)} %bitcast.25), channel_id=1, replica_groups=mesh['ep'=32,'tp'=16] {'tp'}, dimensions={0}, use_global_device_ids=true | all-gather | bytes 974848 | tf_op jit(solution)/shard_map/all_gather | solution.py:332
  60.5 1.3 copy-done
  61.7 1.2 copy-done.1
  63.0 0.7 copy-done.4
  63.7 0.5 early_hidden.1
  64.2 0.0 copy-start.2
  64.2 19.1 %all-gather.1 = bf16[1792,128]{1,0:T(8,128)(2,1)S(1)} all-gather(bf16[112,128]{1,0:T(8,128)(2,1)S(1)} %early_hidden.1), channel_id=3, replica_groups=mesh['ep'=32,'tp'=16] {'tp'}, dimensions={0}, use_global_device_ids=true | all-gather | bytes 487424 | tf_op jit(solution)/shard_map/all_gather | solution.py:334
  83.3 1.0 all-gather.4.cloned.1.call-done
  84.3 7.0 %hidden.1 = bf16[8,400,128]{2,1,0:T(8,128)(2,1)} custom-call(bf16[16,1312,128]{2,1,0:T(8,128)(2,1)} %bitcast.22, f32[1,4096]{1,0:T(1,128)} %bitcast.17, bf16[1,4096,128]{2,1,0:T(8,128)(2,1)} %gate_from.1, bf16[1,4096,128]{2,1,0:T(8,128)(2,1)} %up_from.1), custom_call_target="tpu_custom_call" | custom-call | flops 838860800 | bytes 6500000 | tf_op jit(solution)/shard_map/hidden/pallas_call | solution.py:221
  91.2 27.8 %all_to_all.15.own_ref = bf16[8,400,128]{2,1,0:T(8,128)(2,1)S(1)} all-to-all(bf16[8,400,128]{2,1,0:T(8,128)(2,1)} %hidden.1), channel_id=1, replica_groups={{0,2,4,6,8,10,12,14},{1,3,5,7,9,11,13,15},{16,18,20,22,24,26,28,30},{17..., dimensions={0} | all-to-all | bytes 1638400 | tf_op jit(solution)/shard_map/all_to_all | solution.py:341
  119.0 2.6 %collective-permute-start.1 = (bf16[8,400,128]{2,1,0:T(8,128)(2,1)S(1)}, bf16[8,400,128]{2,1,0:T(8,128)(2,1)S(1)}, u32[]{:S(2)}, u32[]{:S(2)}) collective-permute-start(bf16[8,400,128]{2,1,0:T(8,128)(2,1)S(1)} %all_to_all.15.own_ref), channel_id=1, source_target_pairs={{0,1},{1,0},{2,3},{3,2},{4,5},{5,4},{6,7},{7,6},{8,9},{9,8},{10,11... | collective-permute-start | bytes 2457608 | tf_op jit(solution)/shard_map/ppermute | solution.py:342
  121.6 1.9 %collective-permute-done.1.other_ref = bf16[8,400,128]{2,1,0:T(8,128)(2,1)S(1)} collective-permute-done((bf16[8,400,128]{2,1,0:T(8,128)(2,1)S(1)}, bf16[8,400,128]{2,1,0:T(8,128)(2,1)S(1)}, u32[]{:S(2)}, u32[]{:S(2)}) %collective-permute-start.1) | collective-permute-done | bytes 819232 | tf_op jit(solution)/shard_map/ppermute | solution.py:342
  123.6 1.4 down.1
  125.0 8.8 %all-to-all-start.2 = ((bf16[32,16,256]{2,1,0:T(8,128)(2,1)}), bf16[32,16,256]{2,1,0:T(8,128)(2,1)S(1)}, u32[]{:S(2)}, u32[]{:S(2)}) async-start(bf16[32,16,256]{2,1,0:T(8,128)(2,1)} %bitcast.12), calls=%async_computation.2 | async-start | bytes 524288 | tf_op jit(solution)/shard_map/all_to_all | solution.py:348
  133.8 0.5 shares.1
  134.3 4.9 %mixed.1 = bf16[512,256]{1,0:T(8,128)(2,1)} custom-call(bf16[16,1312,128]{2,1,0:T(8,128)(2,1)} %bitcast.23, bf16[2048,256]{1,0:T(8,128)(2,1)} %weight_ref.1), custom_call_target="tpu_custom_call" | custom-call | flops 536870912 | bytes 3500000 | tf_op jit(solution)/shard_map/mixed/pallas_call | solution.py:256
  139.2 6.2 %all-to-all-done.2 = bf16[32,16,256]{2,1,0:T(8,128)(2,1)S(1)} async-done(((bf16[32,16,256]{2,1,0:T(8,128)(2,1)}), bf16[32,16,256]{2,1,0:T(8,128)(2,1)S(1)}, u32[]{:S(2)}, u32[]{:S(2)}) %all-to-all-start.2) | async-done | bytes 262176 | tf_op jit(solution)/shard_map/all_to_all | solution.py:348
  145.4 0.9 combine.1
  (13 shorter events, 0.0 us)
Async XLA Ops:
  7.2 0.8 copy-start.5
  8.0 0.7 copy-start.6
  9.9 25.0 %all-to-all-start = ((bf16[32,16,256]{2,1,0:T(8,128)(2,1)}), bf16[32,16,256]{2,1,0:T(8,128)(2,1)S(1)}, u32[]{:S(2)}, u32[]{:S(2)}) async-start(bf16[32,16,256]{2,1,0:T(8,128)(2,1)} %bitcast.1), calls=%async_computation | async-start | bytes 524288 | tf_op jit(solution)/shard_map/all_to_all | solution.py:319
  23.6 60.7 %all-gather.4.cloned.1.call-start = ((), (), s32[]{:S(2)}) async-start(), calls=%async_computation.3 | async-start | bytes 5709824 | tf_op jit(solution)/shard_map/all_gather | solution.py:331
  24.3 3.9 %collective-permute-start = (bf16[16,128]{1,0:T(8,128)(2,1)S(1)}, bf16[16,128]{1,0:T(8,128)(2,1)S(1)}, u32[]{:S(2)}, u32[]{:S(2)}) collective-permute-start(bf16[16,128]{1,0:T(8,128)(2,1)S(1)} %slice.15), channel_id=1, source_target_pairs={{0,16},{16,32},{32,48},{48,64},{64,80},{80,96},{96,112},{112,128},... | collective-permute-start | bytes 12296 | tf_op jit(solution)/shard_map/ppermute | solution.py:322
  28.2 0.9 copy-start.3
  60.5 1.3 copy-start
  61.7 1.2 copy-start.1
  63.0 0.7 copy-start.4
  64.2 59.4 %copy-start.2 = (bf16[1,2048,256]{2,1,0:T(8,128)(2,1)S(1)}, bf16[1,2048,256]{2,1,0:T(8,128)(2,1)}, u32[]{:S(2)}) copy-start(bf16[1,2048,256]{2,1,0:T(8,128)(2,1)} %param.17) | copy-start | bytes 3145732
  84.3 49.5 %copy-start.7 = (s32[128,2]{0,1:T(2,128)S(1)}, s32[128,2]{0,1:T(2,128)}, u32[]{:S(2)}) copy-start(s32[128,2]{0,1:T(2,128)} %param.12) | copy-start | bytes 3076
  84.3 49.5 %copy-start.8 = (f32[128,2]{0,1:T(2,128)S(1)}, f32[128,2]{0,1:T(2,128)}, u32[]{:S(2)}) copy-start(f32[128,2]{0,1:T(2,128)} %param.13) | copy-start | bytes 3076
  119.0 4.6 %collective-permute-start.1 = (bf16[8,400,128]{2,1,0:T(8,128)(2,1)S(1)}, bf16[8,400,128]{2,1,0:T(8,128)(2,1)S(1)}, u32[]{:S(2)}, u32[]{:S(2)}) collective-permute-start(bf16[8,400,128]{2,1,0:T(8,128)(2,1)S(1)} %all_to_all.15.own_ref), channel_id=1, source_target_pairs={{0,1},{1,0},{2,3},{3,2},{4,5},{5,4},{6,7},{7,6},{8,9},{9,8},{10,11... | collective-permute-start | bytes 2457608 | tf_op jit(solution)/shard_map/ppermute | solution.py:342
  125.0 20.4 %all-to-all-start.2 = ((bf16[32,16,256]{2,1,0:T(8,128)(2,1)}), bf16[32,16,256]{2,1,0:T(8,128)(2,1)S(1)}, u32[]{:S(2)}, u32[]{:S(2)}) async-start(bf16[32,16,256]{2,1,0:T(8,128)(2,1)} %bitcast.12), calls=%async_computation.2 | async-start | bytes 524288 | tf_op jit(solution)/shard_map/all_to_all | solution.py:348
Sparse Core Ops, SparseCore 0:
  35.8 48.4 all-gather.3

commit v3 on v2

--- a/solution.py
+++ b/solution.py
@@ -16,6 +16,7 @@
 VMEM = pl.BlockSpec(memory_space=pltpu.VMEM)
 SMEM = pl.BlockSpec(memory_space=pltpu.SMEM)
 HBM = pl.BlockSpec(memory_space=pltpu.HBM)
+HOLD = 588 * 2**20 // 10
 EARLY = 112
 
 
@@ -48,9 +49,17 @@
     return hit, first, second, spread
 
 
-def dispatch_kernel(experts, capacity, index_ref, rows_ref, out_ref):
+def dispatch_kernel(experts, capacity, index_from, rows_from, out_ref, index_ref, rows_ref, sems):
+    copies = [
+        pltpu.make_async_copy(index_from, index_ref, sems.at[0]),
+        pltpu.make_async_copy(rows_from, rows_ref, sems.at[1]),
+    ]
+    for copy in copies:
+        copy.start()
+    copies[0].wait()
     hit, _, _, _ = slots_of(index_ref[...], experts, capacity)
     placed = jnp.where(hit, 1.0, 0.0).astype(jnp.bfloat16)
+    copies[1].wait()
     out_ref[...] = dot(placed, rows_ref[...]).astype(out_ref.dtype)
 
 
@@ -58,10 +67,15 @@
     return pl.pallas_call(
         functools.partial(dispatch_kernel, experts, capacity),
         out_shape=jax.ShapeDtypeStruct((experts * capacity, rows.shape[1]), rows.dtype),
-        in_specs=[VMEM, VMEM],
-        out_specs=VMEM,
+        in_specs=[HBM, HBM],
+        out_specs=VMEM,
+        scratch_shapes=[
+            pltpu.VMEM(index.shape, index.dtype),
+            pltpu.VMEM(rows.shape, rows.dtype),
+            pltpu.SemaphoreType.DMA((2,)),
+        ],
         name="dispatch",
-        compiler_params=room(8),
+        compiler_params=room(60),
         cost_estimate=cost(50_000_000, 400_000),
     )(index, rows)
 
@@ -148,31 +162,69 @@
     return (gates / (1.0 + jnp.exp(-gates)) * ups).astype(jnp.bfloat16)
 
 
-def products(rows, gain, gate, up):
-    rows = rows.astype(jnp.float32)
-    scaled = (rows * gain).astype(jnp.bfloat16)
-    square = jnp.square(rows)
-    square = sum(square[:, at : at + 128] for at in range(0, rows.shape[1], 128))
-    return dot(scaled, jnp.concatenate([gate, up], axis=1)), square
-
-
-def early_kernel(rows_ref, gain_ref, gate_ref, up_ref, out_ref):
-    total, square = products(side_by_side(rows_ref), gain_ref[...], gate_ref[0], up_ref[0])
-    out_ref[...] = finish(total, square, gain_ref.shape[1])
-
-
-def early_hidden_of(gathered, gain, gate_weight, up_weight):
+def weights_kernel(gain_from, gate_from, up_from, out_ref, gain_ref, gate_ref, up_ref, sems):
+    copies = [
+        pltpu.make_async_copy(source, held, sems.at[i])
+        for i, (source, held) in enumerate(
+            ((gain_from, gain_ref), (gate_from, gate_ref), (up_from, up_ref))
+        )
+    ]
+    for copy in copies:
+        copy.start()
+    for copy in copies:
+        copy.wait()
+    depth, units = gate_ref.shape[1:]
+    for at in range(0, depth, 128):
+        gain = jnp.broadcast_to(gain_ref[:, at : at + 128], (8, 128)).T[:, 0:1]
+        for first, held in ((0, gate_ref), (units, up_ref)):
+            out_ref[at : at + 128, first : first + units] = (
+                held[0, at : at + 128].astype(jnp.float32) * gain
+            ).astype(out_ref.dtype)
+
+
+def scaled_weights(gain, gate_weight, up_weight):
+    _, depth, units = gate_weight.shape
+    return pl.pallas_call(
+        weights_kernel,
+        out_shape=jax.ShapeDtypeStruct((depth, 2 * units), jnp.bfloat16),
+        in_specs=[HBM, HBM, HBM],
+        out_specs=VMEM,
+        scratch_shapes=[
+            pltpu.VMEM(gain.shape, jnp.float32),
+            pltpu.VMEM(gate_weight.shape, jnp.bfloat16),
+            pltpu.VMEM(up_weight.shape, jnp.bfloat16),
+            pltpu.SemaphoreType.DMA((3,)),
+        ],
+        name="weights",
+        compiler_params=room(61),
+        cost_estimate=cost(3_000_000, 4_200_000),
+    )(gain, gate_weight, up_weight)
+
+
+def products(rows, weight):
+    square = 0.0
+    for at in range(0, rows.shape[1], 128):
+        square = square + jnp.square(rows[:, at : at + 128].astype(jnp.float32))
+    return dot(rows, weight), square
+
+
+def early_kernel(rows_ref, weight_ref, out_ref):
+    total, square = products(side_by_side(rows_ref), weight_ref[...])
+    out_ref[...] = finish(total, square, weight_ref.shape[0])
+
+
+def early_hidden_of(gathered, weight):
     blocks, rows, features = gathered.shape
-    units = gate_weight.shape[2]
+    units = weight.shape[1] // 2
     return pl.pallas_call(
         early_kernel,
         out_shape=jax.ShapeDtypeStruct((rows, units), jnp.bfloat16),
-        in_specs=[VMEM] * 4,
+        in_specs=[VMEM] * 2,
         out_specs=VMEM,
         name="early_hidden",
-        compiler_params=room(24),
+        compiler_params=room(16),
         cost_estimate=cost(4 * rows * blocks * features * units, 3_500_000),
-    )(gathered, gain, gate_weight, up_weight)
+    )(gathered, weight)
 
 
 def fetch(source_ref, first, held, sems):
@@ -184,18 +236,16 @@
     return copies
 
 
-def hidden_kernel(
-    at_once, from_ref, gain_ref, gate_from, up_from, out_ref, held, gate_ref, up_ref, sems, sides
-):
-    weights = [
-        pltpu.make_async_copy(gate_from, gate_ref, sides.at[0]),
-        pltpu.make_async_copy(up_from, up_ref, sides.at[1]),
-    ]
-    for weight in weights:
-        weight.start()
+def hidden_kernel(at_once, from_ref, weight_from, out_ref, held, weight_ref, sems, weight_sems):
     copies = fetch(from_ref, 0, held, sems)
-    for weight in weights:
-        weight.wait()
+    share = weight_ref.shape[0] // (len(copies) // at_once)
+    weights = []
+    for step in range(len(copies) // at_once):
+        part = pl.ds(step * share, share)
+        weights.append(
+            pltpu.make_async_copy(weight_from.at[part], weight_ref.at[part], weight_sems.at[step])
+        )
+        weights[-1].start()
     rows = out_ref.shape[1]
     pieces = held.shape[1] // rows
     depth = at_once * pieces * held.shape[2]
@@ -205,35 +255,34 @@
         for block in range(step * at_once, (step + 1) * at_once):
             copies[block].wait()
             parts += [held[block, i * rows : (i + 1) * rows] for i in range(pieces)]
-        part = slice(step * depth, (step + 1) * depth)
+        weights[step].wait()
         more, squares = products(
-            jnp.concatenate(parts, axis=1), gain_ref[:, part], gate_ref[0, part], up_ref[0, part]
+            jnp.concatenate(parts, axis=1), weight_ref[step * depth : (step + 1) * depth]
         )
         total, square = total + more, square + squares
-    hidden = finish(total, square, gain_ref.shape[1])
+    hidden = finish(total, square, weight_ref.shape[0])
     for copy in range(out_ref.shape[0]):
         out_ref[copy] = hidden
 
 
-def hidden_of(gathered, gain, gate_weight, up_weight, rows, pieces, copies):
+def hidden_of(gathered, weight, rows, pieces, copies):
     blocks, _, lanes = gathered.shape
-    units = gate_weight.shape[2]
-    return pl.pallas_call(
-        functools.partial(hidden_kernel, 4),
-        out_shape=jax.ShapeDtypeStruct((copies, rows, units), jnp.bfloat16),
-        in_specs=[HBM, VMEM, HBM, HBM],
+    depth, both = weight.shape
+    return pl.pallas_call(
+        functools.partial(hidden_kernel, blocks // 2),
+        out_shape=jax.ShapeDtypeStruct((copies, rows, both // 2), jnp.bfloat16),
+        in_specs=[HBM, HBM],
         out_specs=VMEM,
         scratch_shapes=[
             pltpu.VMEM((blocks, pieces * rows, lanes), jnp.bfloat16),
-            pltpu.VMEM(gate_weight.shape, jnp.bfloat16),
-            pltpu.VMEM(up_weight.shape, jnp.bfloat16),
+            pltpu.VMEM(weight.shape, weight.dtype),
             pltpu.SemaphoreType.DMA((blocks,)),
             pltpu.SemaphoreType.DMA((2,)),
         ],
         name="hidden",
-        compiler_params=room(60),
-        cost_estimate=cost(4 * rows * gain.shape[1] * units, 6_500_000),
-    )(gathered, gain, gate_weight, up_weight)
+        compiler_params=pltpu.CompilerParams(vmem_limit_bytes=HOLD),
+        cost_estimate=cost(2 * rows * depth * both, 6_500_000),
+    )(gathered, weight)
 
 
 def mix_kernel(at_once, first, from_ref, weight_ref, out_ref, held, sems):
@@ -314,6 +363,8 @@
     units = gate_weight.shape[2]
     index, share, gain = expert_index.T, route_share.T, norm_gain.reshape(1, -1)
 
+    weight = scaled_weights(gain, gate_weight, up_weight)
+
     outgoing = dispatch(index, expert_input, n_ep, capacity)
     outgoing = outgoing.reshape(n_ep, capacity, features)
     arrived = lax.all_to_all(outgoing, "ep", 0, 0, tiled=True).reshape(n_ep * capacity, features)
@@ -325,15 +376,17 @@
     place = jnp.stack([ep * tokens_mix, tp // (POOL // GROUPS // channels)]).astype(jnp.int32)
     pooled = pool(place, before, mix_input)
 
+    arrived, weight = lax.optimization_barrier((arrived, weight))
+
     late_rows = n_ep * capacity - EARLY
     pieces = features // channels
     sent = [arrived[EARLY:, i * channels : (i + 1) * channels] for i in range(pieces)]
     gathered = lax.all_gather(jnp.concatenate(sent + [pooled], axis=0), "tp", axis=0)
     early = lax.all_gather(arrived[:EARLY], "tp", axis=0)
-    early_hidden = early_hidden_of(early, gain, gate_weight, up_weight)
+    early_hidden = early_hidden_of(early, weight)
     early_hidden = lax.all_gather(early_hidden, "tp", axis=0)
     gathered, early_hidden = lax.optimization_barrier((gathered, early_hidden))
-    hidden = hidden_of(gathered, gain, gate_weight, up_weight, late_rows, pieces, chips)
+    hidden = hidden_of(gathered, weight, late_rows, pieces, chips)
     mixed_rows = mixed_of(gathered, mix_weight, pieces * late_rows, tokens_mix)
 
     columns_of_chips = [[chip * 2 + core for chip in range(chips)] for core in range(2)]

time: 154 us -> 152 us (0.987)
  Pallas kernels: 17.1 us -> 20.2 us
  local copies, waits for them, and re-layouts: 6.36 us -> 3.27 us
    all_to_all x1, waiting for transfers between devices: 5.03 us -> 1.53 us  [shards(): lax.all_to_all(outgoing, 'ep', 0, 0, tiled=True)]
    unnamed x18 -> x10, local copies, waits for them, and re-layouts: 5.65 us -> 2.56 us
    all_gather x1, waiting for transfers between devices: 0.97 us -> 3.66 us  [shards(): lax.all_gather(jnp.concatenate(sent + [pooled], axis=0), 'tp', axis=0)]
    pallas_call x1 -> x2, Pallas kernels: 6.97 us -> 9.3 us  [the longest x1 5.17 us: hidden_of(): pl.pallas_call(functools.partial(hidden_kernel, blocks // 2), out_shape=j...]
  transfers between devices with their start and end apart: 5 -> 5, of which waited for: 5 -> 4; matrix products, arithmetic and copies ran while one was open for 1% -> 1% of each run, Pallas kernels for 4% -> 7%
where the time goes in v3:
time: 152 us
  blocking collectives  70.7 us (47%)
  starting transfers between devices  29.1 us (19%)
  Pallas kernels  20.2 us (13%)
  between operations  14.2 us (9%)
  waiting for transfers between devices  13.3 us (9%)
  local copies, waits for them, and re-layouts  3.27 us (2%)
    all_to_all x1, blocking collectives, shards(): lax.all_to_all(hidden, 'tp', 0, 0, tiled=True, axis_index_groups=columns_...  27.2 us
    all_gather x1, blocking collectives, shards(): early = lax.all_gather(arrived[:EARLY], 'tp', axis=0)  25.1 us
    all_gather x1, blocking collectives, shards(): early_hidden = lax.all_gather(early_hidden, 'tp', axis=0)  18.4 us
    all_to_all x1, starting transfers between devices, shards(): lax.all_to_all(outgoing, 'ep', 0, 0, tiled=True)  13.7 us
    all_to_all x1, starting transfers between devices, shards(): lax.all_to_all(produced.reshape(n_ep, capacity, produced.shape[1]), 'ep',...  9.12 us
    all_to_all x1, waiting for transfers between devices, shards(): lax.all_to_all(produced.reshape(n_ep, capacity, produced.shape[1]), 'ep',...  6.2 us
    pallas_call x1, Pallas kernels, hidden_of(): pl.pallas_call(functools.partial(hidden_kernel, blocks // 2), out_shape=j...  5.17 us
    pallas_call x1, Pallas kernels, mixed_of(): pl.pallas_call(functools.partial(mix_kernel, 4, first), out_shape=jax.Sha...  4.87 us
  transfers between devices with their start and end apart: 5, of which 4 were waited for; matrix products, arithmetic and copies ran while one was open for 1% of the time, Pallas kernels for 7%

profile of v3, /device:TPU:1, one launch (start us, length us, event | category | flops | bytes accessed | tf_op | source)
XLA Modules:
  0.0 151.6 jit_solution(15587133960378753119)
XLA Ops:
  7.2 2.0 %dispatch.1 = bf16[512,256]{1,0:T(8,128)(2,1)} custom-call(s32[2,128]{1,0:T(2,128)} %bitcast.18, bf16[128,256]{1,0:T(8,128)(2,1)} %rows_from.1), custom_call_target="tpu_custom_call" | custom-call | flops 50000000 | bytes 400000 | tf_op jit(solution)/shard_map/dispatch/pallas_call | solution.py:67
  9.1 13.7 %all-to-all-start = ((bf16[32,16,256]{2,1,0:T(8,128)(2,1)}), bf16[32,16,256]{2,1,0:T(8,128)(2,1)S(1)}, u32[]{:S(2)}, u32[]{:S(2)}) async-start(bf16[32,16,256]{2,1,0:T(8,128)(2,1)} %bitcast.25), calls=%async_computation | async-start | bytes 524288 | tf_op jit(solution)/shard_map/all_to_all | solution.py:370
  22.9 0.0 all-gather.5.cloned.1.call-start
  22.9 0.7 slice.14
  23.6 3.1 %collective-permute-start = (bf16[16,128]{1,0:T(8,128)(2,1)S(1)}, bf16[16,128]{1,0:T(8,128)(2,1)S(1)}, u32[]{:S(2)}, u32[]{:S(2)}) collective-permute-start(bf16[16,128]{1,0:T(8,128)(2,1)S(1)} %slice.14), channel_id=1, source_target_pairs={{0,16},{16,32},{32,48},{48,64},{64,80},{80,96},{96,112},{112,128},... | collective-permute-start | bytes 12296 | tf_op jit(solution)/shard_map/ppermute | solution.py:373
  26.7 0.1 pad_add_fusion.place_ref
  26.8 4.1 %weights.1.weight_ref.weight_from = bf16[4096,256]{1,0:T(8,128)(2,1)} custom-call(f32[1,4096]{1,0:T(1,128)} %bitcast.26, bf16[1,4096,128]{2,1,0:T(8,128)(2,1)} %gate_from.1, bf16[1,4096,128]{2,1,0:T(8,128)(2,1)} %up_from.1), custom_call_target="tpu_custom_call" | custom-call | flops 3000000 | bytes 4200000 | tf_op jit(solution)/shard_map/weights/pallas_call | solution.py:187
  31.0 0.0 collective-permute-done.before_ref
  31.0 0.0 copy-start.2
  31.0 0.9 copy-done.2
  31.9 0.8 pool.1
  32.6 1.5 %all-to-all-done = bf16[32,16,256]{2,1,0:T(8,128)(2,1)S(1)} async-done(((bf16[32,16,256]{2,1,0:T(8,128)(2,1)}), bf16[32,16,256]{2,1,0:T(8,128)(2,1)S(1)}, u32[]{:S(2)}, u32[]{:S(2)}) %all-to-all-start) | async-done | bytes 262176 | tf_op jit(solution)/shard_map/all_to_all | solution.py:370
  34.2 0.8 pad_maximum_fusion
  34.9 0.0 all-gather.5.cloned.1.call-update
  35.0 25.1 %all-gather.1 = bf16[1792,256]{1,0:T(8,128)(2,1)S(1)} all-gather(bf16[112,256]{1,0:T(8,128)(2,1)S(1)} %slice.15), channel_id=3, replica_groups=mesh['ep'=32,'tp'=16] {'tp'}, dimensions={0}, use_global_device_ids=true | all-gather | bytes 974848 | tf_op jit(solution)/shard_map/all_gather | solution.py:385
  60.1 1.6 %copy-done = bf16[4096,256]{1,0:T(8,128)(2,1)S(1)} copy-done((bf16[4096,256]{1,0:T(8,128)(2,1)S(1)}, bf16[4096,256]{1,0:T(8,128)(2,1)}, u32[]{:S(2)}) %copy-start) | copy-done | bytes 2097176
  61.7 0.5 early_hidden.1
  62.3 0.0 copy-start.1
  62.3 18.4 %all-gather.2 = bf16[1792,128]{1,0:T(8,128)(2,1)S(1)} all-gather(bf16[112,128]{1,0:T(8,128)(2,1)S(1)} %early_hidden.1), channel_id=4, replica_groups=mesh['ep'=32,'tp'=16] {'tp'}, dimensions={0}, use_global_device_ids=true | all-gather | bytes 487424 | tf_op jit(solution)/shard_map/all_gather | solution.py:387
  80.6 3.7 %all-gather.5.cloned.1.call-done = bf16[20992,128]{1,0:T(8,128)(2,1)} async-done(((bf16[1312,128]{1,0:T(8,128)(2,1)}), bf16[20992,128]{1,0:T(8,128)(2,1)}) %all-gather.5.cloned.1.call-update) | async-done | bytes 5373968 | tf_op jit(solution)/shard_map/all_gather | solution.py:384
  84.3 5.2 %hidden.1 = bf16[8,400,128]{2,1,0:T(8,128)(2,1)} custom-call(bf16[16,1312,128]{2,1,0:T(8,128)(2,1)} %bitcast.21, bf16[4096,256]{1,0:T(8,128)(2,1)} %weights.1.weight_ref.weight_from), custom_call_target="tpu_custom_call" | custom-call | flops 838860800 | bytes 6500000 | tf_op jit(solution)/shard_map/hidden/pallas_call | solution.py:271
  89.5 27.2 %all_to_all.15.own_ref = bf16[8,400,128]{2,1,0:T(8,128)(2,1)S(1)} all-to-all(bf16[8,400,128]{2,1,0:T(8,128)(2,1)} %hidden.1), channel_id=1, replica_groups={{0,2,4,6,8,10,12,14},{1,3,5,7,9,11,13,15},{16,18,20,22,24,26,28,30},{17..., dimensions={0} | all-to-all | bytes 1638400 | tf_op jit(solution)/shard_map/all_to_all | solution.py:394
  116.7 3.1 %collective-permute-start.1 = (bf16[8,400,128]{2,1,0:T(8,128)(2,1)S(1)}, bf16[8,400,128]{2,1,0:T(8,128)(2,1)S(1)}, u32[]{:S(2)}, u32[]{:S(2)}) collective-permute-start(bf16[8,400,128]{2,1,0:T(8,128)(2,1)S(1)} %all_to_all.15.own_ref), channel_id=1, source_target_pairs={{0,1},{1,0},{2,3},{3,2},{4,5},{5,4},{6,7},{7,6},{8,9},{9,8},{10,11... | collective-permute-start | bytes 2457608 | tf_op jit(solution)/shard_map/ppermute | solution.py:395
  119.8 1.9 %collective-permute-done.1.other_ref = bf16[8,400,128]{2,1,0:T(8,128)(2,1)S(1)} collective-permute-done((bf16[8,400,128]{2,1,0:T(8,128)(2,1)S(1)}, bf16[8,400,128]{2,1,0:T(8,128)(2,1)S(1)}, u32[]{:S(2)}, u32[]{:S(2)}) %collective-permute-start.1) | collective-permute-done | bytes 819232 | tf_op jit(solution)/shard_map/ppermute | solution.py:395
  121.7 1.4 down.1
  123.2 9.1 %all-to-all-start.2 = ((bf16[32,16,256]{2,1,0:T(8,128)(2,1)}), bf16[32,16,256]{2,1,0:T(8,128)(2,1)S(1)}, u32[]{:S(2)}, u32[]{:S(2)}) async-start(bf16[32,16,256]{2,1,0:T(8,128)(2,1)} %bitcast.12), calls=%async_computation.2 | async-start | bytes 524288 | tf_op jit(solution)/shard_map/all_to_all | solution.py:401
  132.3 0.0 copy-done.3
  132.3 0.0 copy-done.4
  132.3 0.5 shares.1
  132.8 4.9 %mixed.1 = bf16[512,256]{1,0:T(8,128)(2,1)} custom-call(bf16[16,1312,128]{2,1,0:T(8,128)(2,1)} %bitcast.22, bf16[2048,256]{1,0:T(8,128)(2,1)} %weight_ref.1), custom_call_target="tpu_custom_call" | custom-call | flops 536870912 | bytes 3500000 | tf_op jit(solution)/shard_map/mixed/pallas_call | solution.py:305
  137.7 6.2 %all-to-all-done.2 = bf16[32,16,256]{2,1,0:T(8,128)(2,1)S(1)} async-done(((bf16[32,16,256]{2,1,0:T(8,128)(2,1)}), bf16[32,16,256]{2,1,0:T(8,128)(2,1)S(1)}, u32[]{:S(2)}, u32[]{:S(2)}) %all-to-all-start.2) | async-done | bytes 262176 | tf_op jit(solution)/shard_map/all_to_all | solution.py:401
  143.9 0.9 combine.1
  (6 shorter events, 0.0 us)
Async XLA Ops:
  9.1 25.0 %all-to-all-start = ((bf16[32,16,256]{2,1,0:T(8,128)(2,1)}), bf16[32,16,256]{2,1,0:T(8,128)(2,1)S(1)}, u32[]{:S(2)}, u32[]{:S(2)}) async-start(bf16[32,16,256]{2,1,0:T(8,128)(2,1)} %bitcast.25), calls=%async_computation | async-start | bytes 524288 | tf_op jit(solution)/shard_map/all_to_all | solution.py:370
  22.9 61.4 %all-gather.5.cloned.1.call-start = ((), (), s32[]{:S(2)}) async-start(), calls=%async_computation.3 | async-start | bytes 5709824 | tf_op jit(solution)/shard_map/all_gather | solution.py:384
  23.6 7.4 %collective-permute-start = (bf16[16,128]{1,0:T(8,128)(2,1)S(1)}, bf16[16,128]{1,0:T(8,128)(2,1)S(1)}, u32[]{:S(2)}, u32[]{:S(2)}) collective-permute-start(bf16[16,128]{1,0:T(8,128)(2,1)S(1)} %slice.14), channel_id=1, source_target_pairs={{0,16},{16,32},{32,48},{48,64},{64,80},{80,96},{96,112},{112,128},... | collective-permute-start | bytes 12296 | tf_op jit(solution)/shard_map/ppermute | solution.py:373
  31.0 0.9 copy-start.2
  60.1 1.6 %copy-start = (bf16[4096,256]{1,0:T(8,128)(2,1)S(1)}, bf16[4096,256]{1,0:T(8,128)(2,1)}, u32[]{:S(2)}) copy-start(bf16[4096,256]{1,0:T(8,128)(2,1)} %weights.1.weight_ref.weight_from) | copy-start | bytes 6291460
  62.3 59.5 %copy-start.1 = (bf16[1,2048,256]{2,1,0:T(8,128)(2,1)S(1)}, bf16[1,2048,256]{2,1,0:T(8,128)(2,1)}, u32[]{:S(2)}) copy-start(bf16[1,2048,256]{2,1,0:T(8,128)(2,1)} %param.17) | copy-start | bytes 3145732
  84.3 48.0 %copy-start.3 = (s32[128,2]{0,1:T(2,128)S(1)}, s32[128,2]{0,1:T(2,128)}, u32[]{:S(2)}) copy-start(s32[128,2]{0,1:T(2,128)} %param.12) | copy-start | bytes 3076
  84.3 48.0 %copy-start.4 = (f32[128,2]{0,1:T(2,128)S(1)}, f32[128,2]{0,1:T(2,128)}, u32[]{:S(2)}) copy-start(f32[128,2]{0,1:T(2,128)} %param.13) | copy-start | bytes 3076
  116.7 5.0 %collective-permute-start.1 = (bf16[8,400,128]{2,1,0:T(8,128)(2,1)S(1)}, bf16[8,400,128]{2,1,0:T(8,128)(2,1)S(1)}, u32[]{:S(2)}, u32[]{:S(2)}) collective-permute-start(bf16[8,400,128]{2,1,0:T(8,128)(2,1)S(1)} %all_to_all.15.own_ref), channel_id=1, source_target_pairs={{0,1},{1,0},{2,3},{3,2},{4,5},{5,4},{6,7},{7,6},{8,9},{9,8},{10,11... | collective-permute-start | bytes 2457608 | tf_op jit(solution)/shard_map/ppermute | solution.py:395
  123.2 20.7 %all-to-all-start.2 = ((bf16[32,16,256]{2,1,0:T(8,128)(2,1)}), bf16[32,16,256]{2,1,0:T(8,128)(2,1)S(1)}, u32[]{:S(2)}, u32[]{:S(2)}) async-start(bf16[32,16,256]{2,1,0:T(8,128)(2,1)} %bitcast.12), calls=%async_computation.2 | async-start | bytes 524288 | tf_op jit(solution)/shard_map/all_to_all | solution.py:401
Sparse Core Ops, SparseCore 0:
  35.1 49.1 all-gather.4

commit v4 on v2

--- a/solution.py
+++ b/solution.py
@@ -16,6 +16,7 @@
 VMEM = pl.BlockSpec(memory_space=pltpu.VMEM)
 SMEM = pl.BlockSpec(memory_space=pltpu.SMEM)
 HBM = pl.BlockSpec(memory_space=pltpu.HBM)
+HOLD = 588 * 2**20 // 10
 EARLY = 112
 
 
@@ -48,9 +49,17 @@
     return hit, first, second, spread
 
 
-def dispatch_kernel(experts, capacity, index_ref, rows_ref, out_ref):
+def dispatch_kernel(experts, capacity, index_from, rows_from, out_ref, index_ref, rows_ref, sems):
+    copies = [
+        pltpu.make_async_copy(index_from, index_ref, sems.at[0]),
+        pltpu.make_async_copy(rows_from, rows_ref, sems.at[1]),
+    ]
+    for copy in copies:
+        copy.start()
+    copies[0].wait()
     hit, _, _, _ = slots_of(index_ref[...], experts, capacity)
     placed = jnp.where(hit, 1.0, 0.0).astype(jnp.bfloat16)
+    copies[1].wait()
     out_ref[...] = dot(placed, rows_ref[...]).astype(out_ref.dtype)
 
 
@@ -58,10 +67,15 @@
     return pl.pallas_call(
         functools.partial(dispatch_kernel, experts, capacity),
         out_shape=jax.ShapeDtypeStruct((experts * capacity, rows.shape[1]), rows.dtype),
-        in_specs=[VMEM, VMEM],
-        out_specs=VMEM,
+        in_specs=[HBM, HBM],
+        out_specs=VMEM,
+        scratch_shapes=[
+            pltpu.VMEM(index.shape, index.dtype),
+            pltpu.VMEM(rows.shape, rows.dtype),
+            pltpu.SemaphoreType.DMA((2,)),
+        ],
         name="dispatch",
-        compiler_params=room(8),
+        compiler_params=room(60),
         cost_estimate=cost(50_000_000, 400_000),
     )(index, rows)
 
@@ -188,14 +202,12 @@
     at_once, from_ref, gain_ref, gate_from, up_from, out_ref, held, gate_ref, up_ref, sems, sides
 ):
     weights = [
-        pltpu.make_async_copy(gate_from, gate_ref, sides.at[0]),
-        pltpu.make_async_copy(up_from, up_ref, sides.at[1]),
+        pltpu.make_async_copy(source, kept, sides.at[i])
+        for i, (source, kept) in enumerate(((gate_from, gate_ref), (up_from, up_ref)))
     ]
     for weight in weights:
         weight.start()
     copies = fetch(from_ref, 0, held, sems)
-    for weight in weights:
-        weight.wait()
     rows = out_ref.shape[1]
     pieces = held.shape[1] // rows
     depth = at_once * pieces * held.shape[2]
@@ -205,6 +217,9 @@
         for block in range(step * at_once, (step + 1) * at_once):
             copies[block].wait()
             parts += [held[block, i * rows : (i + 1) * rows] for i in range(pieces)]
+        if step == 0:
+            for weight in weights:
+                weight.wait()
         part = slice(step * depth, (step + 1) * depth)
         more, squares = products(
             jnp.concatenate(parts, axis=1), gain_ref[:, part], gate_ref[0, part], up_ref[0, part]
@@ -219,7 +234,7 @@
     blocks, _, lanes = gathered.shape
     units = gate_weight.shape[2]
     return pl.pallas_call(
-        functools.partial(hidden_kernel, 4),
+        functools.partial(hidden_kernel, blocks // 2),
         out_shape=jax.ShapeDtypeStruct((copies, rows, units), jnp.bfloat16),
         in_specs=[HBM, VMEM, HBM, HBM],
         out_specs=VMEM,
@@ -231,7 +246,7 @@
             pltpu.SemaphoreType.DMA((2,)),
         ],
         name="hidden",
-        compiler_params=room(60),
+        compiler_params=pltpu.CompilerParams(vmem_limit_bytes=HOLD),
         cost_estimate=cost(4 * rows * gain.shape[1] * units, 6_500_000),
     )(gathered, gain, gate_weight, up_weight)
 

time: 154 us -> 152 us (0.987)
    unnamed x18 -> x14, local copies, waits for them, and re-layouts: 5.65 us -> 4.14 us
where the time goes in v4:
time: 152 us
  blocking collectives  71.6 us (47%)
  starting transfers between devices  28.3 us (19%)
  Pallas kernels  17 us (11%)
  waiting for transfers between devices  14.8 us (10%)
  between operations  14.2 us (9%)
  local copies, waits for them, and re-layouts  4.85 us (3%)
    all_to_all x1, blocking collectives, shards(): lax.all_to_all(hidden, 'tp', 0, 0, tiled=True, axis_index_groups=columns_...  27.7 us
    all_gather x1, blocking collectives, shards(): early = lax.all_gather(arrived[:EARLY], 'tp', axis=0)  24.8 us
    all_gather x1, blocking collectives, shards(): early_hidden = lax.all_gather(early_hidden, 'tp', axis=0)  19.1 us
    all_to_all x1, starting transfers between devices, shards(): lax.all_to_all(outgoing, 'ep', 0, 0, tiled=True)  13.7 us
    all_to_all x1, starting transfers between devices, shards(): lax.all_to_all(produced.reshape(n_ep, capacity, produced.shape[1]), 'ep',...  8.79 us
    all_to_all x1, waiting for transfers between devices, shards(): lax.all_to_all(produced.reshape(n_ep, capacity, produced.shape[1]), 'ep',...  6.2 us
    pallas_call x1, Pallas kernels, hidden_of(): pl.pallas_call(functools.partial(hidden_kernel, blocks // 2), out_shape=j...  6.14 us
    all_to_all x1, waiting for transfers between devices, shards(): lax.all_to_all(outgoing, 'ep', 0, 0, tiled=True)  5.03 us
  transfers between devices with their start and end apart: 5, of which 5 were waited for; matrix products, arithmetic and copies ran while one was open for 1% of the time, Pallas kernels for 4%

profile of v4, /device:TPU:1, one launch (start us, length us, event | category | flops | bytes accessed | tf_op | source)
XLA Modules:
  0.0 151.5 jit_solution(10832599829169144287)
XLA Ops:
  7.2 2.0 %dispatch.1 = bf16[512,256]{1,0:T(8,128)(2,1)} custom-call(s32[2,128]{1,0:T(2,128)} %bitcast.19, bf16[128,256]{1,0:T(8,128)(2,1)} %rows_from.1), custom_call_target="tpu_custom_call" | custom-call | flops 50000000 | bytes 400000 | tf_op jit(solution)/shard_map/dispatch/pallas_call | solution.py:67
  9.1 13.7 %all-to-all-start = ((bf16[32,16,256]{2,1,0:T(8,128)(2,1)}), bf16[32,16,256]{2,1,0:T(8,128)(2,1)S(1)}, u32[]{:S(2)}, u32[]{:S(2)}) async-start(bf16[32,16,256]{2,1,0:T(8,128)(2,1)} %bitcast.25), calls=%async_computation | async-start | bytes 524288 | tf_op jit(solution)/shard_map/all_to_all | solution.py:334
  22.9 0.0 all-gather.4.cloned.1.call-start
  22.9 0.7 slice.15
  23.6 3.1 %collective-permute-start = (bf16[16,128]{1,0:T(8,128)(2,1)S(1)}, bf16[16,128]{1,0:T(8,128)(2,1)S(1)}, u32[]{:S(2)}, u32[]{:S(2)}) collective-permute-start(bf16[16,128]{1,0:T(8,128)(2,1)S(1)} %slice.15), channel_id=1, source_target_pairs={{0,16},{16,32},{32,48},{48,64},{64,80},{80,96},{96,112},{112,128},... | collective-permute-start | bytes 12296 | tf_op jit(solution)/shard_map/ppermute | solution.py:337
  26.7 0.1 pad_add_fusion.place_ref
  26.8 0.6 collective-permute-done.before_ref
  27.5 0.9 copy-done.3
  28.4 0.8 pool.1
  29.1 5.0 %all-to-all-done = bf16[32,16,256]{2,1,0:T(8,128)(2,1)S(1)} async-done(((bf16[32,16,256]{2,1,0:T(8,128)(2,1)}), bf16[32,16,256]{2,1,0:T(8,128)(2,1)S(1)}, u32[]{:S(2)}, u32[]{:S(2)}) %all-to-all-start) | async-done | bytes 262176 | tf_op jit(solution)/shard_map/all_to_all | solution.py:334
  34.2 0.8 pad_maximum_fusion
  35.0 0.0 all-gather.4.cloned.1.call-update
  35.0 24.8 %all_gather.21.rows_ref = bf16[16,112,256]{2,1,0:T(8,128)(2,1)S(1)} all-gather(bf16[1,112,256]{2,1,0:T(8,128)(2,1)S(1)} %bitcast.26), channel_id=1, replica_groups=mesh['ep'=32,'tp'=16] {'tp'}, dimensions={0}, use_global_device_ids=true | all-gather | bytes 974848 | tf_op jit(solution)/shard_map/all_gather | solution.py:347
  59.8 1.3 copy-done
  61.0 1.2 copy-done.1
  62.3 0.7 copy-done.4
  63.0 0.5 early_hidden.1
  63.5 0.0 copy-start.2
  63.5 19.1 %all-gather.1 = bf16[1792,128]{1,0:T(8,128)(2,1)S(1)} all-gather(bf16[112,128]{1,0:T(8,128)(2,1)S(1)} %early_hidden.1), channel_id=3, replica_groups=mesh['ep'=32,'tp'=16] {'tp'}, dimensions={0}, use_global_device_ids=true | all-gather | bytes 487424 | tf_op jit(solution)/shard_map/all_gather | solution.py:349
  82.6 1.0 all-gather.4.cloned.1.call-done
  83.6 6.1 %hidden.1 = bf16[8,400,128]{2,1,0:T(8,128)(2,1)} custom-call(bf16[16,1312,128]{2,1,0:T(8,128)(2,1)} %bitcast.22, f32[1,4096]{1,0:T(1,128)} %bitcast.17, bf16[1,4096,128]{2,1,0:T(8,128)(2,1)} %gate_from.1, bf16[1,4096,128]{2,1,0:T(8,128)(2,1)} %up_from.1), custom_call_target="tpu_custom_call" | custom-call | flops 838860800 | bytes 6500000 | tf_op jit(solution)/shard_map/hidden/pallas_call | solution.py:236
  89.7 27.7 %all_to_all.15.own_ref = bf16[8,400,128]{2,1,0:T(8,128)(2,1)S(1)} all-to-all(bf16[8,400,128]{2,1,0:T(8,128)(2,1)} %hidden.1), channel_id=1, replica_groups={{0,2,4,6,8,10,12,14},{1,3,5,7,9,11,13,15},{16,18,20,22,24,26,28,30},{17..., dimensions={0} | all-to-all | bytes 1638400 | tf_op jit(solution)/shard_map/all_to_all | solution.py:356
  117.4 2.6 %collective-permute-start.1 = (bf16[8,400,128]{2,1,0:T(8,128)(2,1)S(1)}, bf16[8,400,128]{2,1,0:T(8,128)(2,1)S(1)}, u32[]{:S(2)}, u32[]{:S(2)}) collective-permute-start(bf16[8,400,128]{2,1,0:T(8,128)(2,1)S(1)} %all_to_all.15.own_ref), channel_id=1, source_target_pairs={{0,1},{1,0},{2,3},{3,2},{4,5},{5,4},{6,7},{7,6},{8,9},{9,8},{10,11... | collective-permute-start | bytes 2457608 | tf_op jit(solution)/shard_map/ppermute | solution.py:357
  120.1 1.9 %collective-permute-done.1.other_ref = bf16[8,400,128]{2,1,0:T(8,128)(2,1)S(1)} collective-permute-done((bf16[8,400,128]{2,1,0:T(8,128)(2,1)S(1)}, bf16[8,400,128]{2,1,0:T(8,128)(2,1)S(1)}, u32[]{:S(2)}, u32[]{:S(2)}) %collective-permute-start.1) | collective-permute-done | bytes 819232 | tf_op jit(solution)/shard_map/ppermute | solution.py:357
  122.0 0.0 copy-done.2
  122.0 1.4 down.1
  123.4 8.8 %all-to-all-start.2 = ((bf16[32,16,256]{2,1,0:T(8,128)(2,1)}), bf16[32,16,256]{2,1,0:T(8,128)(2,1)S(1)}, u32[]{:S(2)}, u32[]{:S(2)}) async-start(bf16[32,16,256]{2,1,0:T(8,128)(2,1)} %bitcast.12), calls=%async_computation.2 | async-start | bytes 524288 | tf_op jit(solution)/shard_map/all_to_all | solution.py:363
  132.2 0.0 copy-done.5
  132.3 0.5 shares.1
  132.8 4.9 %mixed.1 = bf16[512,256]{1,0:T(8,128)(2,1)} custom-call(bf16[16,1312,128]{2,1,0:T(8,128)(2,1)} %bitcast.23, bf16[2048,256]{1,0:T(8,128)(2,1)} %weight_ref.1), custom_call_target="tpu_custom_call" | custom-call | flops 536870912 | bytes 3500000 | tf_op jit(solution)/shard_map/mixed/pallas_call | solution.py:271
  137.6 6.2 %all-to-all-done.2 = bf16[32,16,256]{2,1,0:T(8,128)(2,1)S(1)} async-done(((bf16[32,16,256]{2,1,0:T(8,128)(2,1)}), bf16[32,16,256]{2,1,0:T(8,128)(2,1)S(1)}, u32[]{:S(2)}, u32[]{:S(2)}) %all-to-all-start.2) | async-done | bytes 262176 | tf_op jit(solution)/shard_map/all_to_all | solution.py:363
  143.8 0.9 combine.1
  (9 shorter events, 0.0 us)
Async XLA Ops:
  9.1 25.0 %all-to-all-start = ((bf16[32,16,256]{2,1,0:T(8,128)(2,1)}), bf16[32,16,256]{2,1,0:T(8,128)(2,1)S(1)}, u32[]{:S(2)}, u32[]{:S(2)}) async-start(bf16[32,16,256]{2,1,0:T(8,128)(2,1)} %bitcast.25), calls=%async_computation | async-start | bytes 524288 | tf_op jit(solution)/shard_map/all_to_all | solution.py:334
  22.9 60.7 %all-gather.4.cloned.1.call-start = ((), (), s32[]{:S(2)}) async-start(), calls=%async_computation.3 | async-start | bytes 5709824 | tf_op jit(solution)/shard_map/all_gather | solution.py:346
  23.6 3.9 %collective-permute-start = (bf16[16,128]{1,0:T(8,128)(2,1)S(1)}, bf16[16,128]{1,0:T(8,128)(2,1)S(1)}, u32[]{:S(2)}, u32[]{:S(2)}) collective-permute-start(bf16[16,128]{1,0:T(8,128)(2,1)S(1)} %slice.15), channel_id=1, source_target_pairs={{0,16},{16,32},{32,48},{48,64},{64,80},{80,96},{96,112},{112,128},... | collective-permute-start | bytes 12296 | tf_op jit(solution)/shard_map/ppermute | solution.py:337
  27.5 0.9 copy-start.3
  59.8 1.3 copy-start
  61.0 1.2 copy-start.1
  62.3 0.7 copy-start.4
  63.5 58.5 %copy-start.2 = (bf16[1,2048,256]{2,1,0:T(8,128)(2,1)S(1)}, bf16[1,2048,256]{2,1,0:T(8,128)(2,1)}, u32[]{:S(2)}) copy-start(bf16[1,2048,256]{2,1,0:T(8,128)(2,1)} %param.17) | copy-start | bytes 3145732
  83.5 48.7 %copy-start.5 = (s32[128,2]{0,1:T(2,128)S(1)}, s32[128,2]{0,1:T(2,128)}, u32[]{:S(2)}) copy-start(s32[128,2]{0,1:T(2,128)} %param.12) | copy-start | bytes 3076
  83.6 48.7 %copy-start.6 = (f32[128,2]{0,1:T(2,128)S(1)}, f32[128,2]{0,1:T(2,128)}, u32[]{:S(2)}) copy-start(f32[128,2]{0,1:T(2,128)} %param.13) | copy-start | bytes 3076
  117.4 4.6 %collective-permute-start.1 = (bf16[8,400,128]{2,1,0:T(8,128)(2,1)S(1)}, bf16[8,400,128]{2,1,0:T(8,128)(2,1)S(1)}, u32[]{:S(2)}, u32[]{:S(2)}) collective-permute-start(bf16[8,400,128]{2,1,0:T(8,128)(2,1)S(1)} %all_to_all.15.own_ref), channel_id=1, source_target_pairs={{0,1},{1,0},{2,3},{3,2},{4,5},{5,4},{6,7},{7,6},{8,9},{9,8},{10,11... | collective-permute-start | bytes 2457608 | tf_op jit(solution)/shard_map/ppermute | solution.py:357
  123.4 20.4 %all-to-all-start.2 = ((bf16[32,16,256]{2,1,0:T(8,128)(2,1)}), bf16[32,16,256]{2,1,0:T(8,128)(2,1)S(1)}, u32[]{:S(2)}, u32[]{:S(2)}) async-start(bf16[32,16,256]{2,1,0:T(8,128)(2,1)} %bitcast.12), calls=%async_computation.2 | async-start | bytes 524288 | tf_op jit(solution)/shard_map/all_to_all | solution.py:363
Sparse Core Ops, SparseCore 0:
  35.1 48.4 all-gather.3

commit v5 on v4

--- a/solution.py
+++ b/solution.py
@@ -16,7 +16,6 @@
 VMEM = pl.BlockSpec(memory_space=pltpu.VMEM)
 SMEM = pl.BlockSpec(memory_space=pltpu.SMEM)
 HBM = pl.BlockSpec(memory_space=pltpu.HBM)
-HOLD = 588 * 2**20 // 10
 EARLY = 112
 
 
@@ -199,14 +198,8 @@
 
 
 def hidden_kernel(
-    at_once, from_ref, gain_ref, gate_from, up_from, out_ref, held, gate_ref, up_ref, sems, sides
+    at_once, from_ref, gain_ref, gate_ref, up_ref, out_ref, held, sems
 ):
-    weights = [
-        pltpu.make_async_copy(source, kept, sides.at[i])
-        for i, (source, kept) in enumerate(((gate_from, gate_ref), (up_from, up_ref)))
-    ]
-    for weight in weights:
-        weight.start()
     copies = fetch(from_ref, 0, held, sems)
     rows = out_ref.shape[1]
     pieces = held.shape[1] // rows
@@ -217,9 +210,6 @@
         for block in range(step * at_once, (step + 1) * at_once):
             copies[block].wait()
             parts += [held[block, i * rows : (i + 1) * rows] for i in range(pieces)]
-        if step == 0:
-            for weight in weights:
-                weight.wait()
         part = slice(step * depth, (step + 1) * depth)
         more, squares = products(
             jnp.concatenate(parts, axis=1), gain_ref[:, part], gate_ref[0, part], up_ref[0, part]
@@ -236,19 +226,16 @@
     return pl.pallas_call(
         functools.partial(hidden_kernel, blocks // 2),
         out_shape=jax.ShapeDtypeStruct((copies, rows, units), jnp.bfloat16),
-        in_specs=[HBM, VMEM, HBM, HBM],
+        in_specs=[HBM, VMEM, VMEM, VMEM],
         out_specs=VMEM,
         scratch_shapes=[
             pltpu.VMEM((blocks, pieces * rows, lanes), jnp.bfloat16),
-            pltpu.VMEM(gate_weight.shape, jnp.bfloat16),
-            pltpu.VMEM(up_weight.shape, jnp.bfloat16),
             pltpu.SemaphoreType.DMA((blocks,)),
-            pltpu.SemaphoreType.DMA((2,)),
         ],
         name="hidden",
-        compiler_params=pltpu.CompilerParams(vmem_limit_bytes=HOLD),
+        compiler_params=room(28),
         cost_estimate=cost(4 * rows * gain.shape[1] * units, 6_500_000),
-    )(gathered, gain, gate_weight, up_weight)
+    )(pltpu.with_memory_space_constraint(gathered, pltpu.HBM), gain, gate_weight, up_weight)
 
 
 def mix_kernel(at_once, first, from_ref, weight_ref, out_ref, held, sems):
@@ -278,9 +265,9 @@
             pltpu.SemaphoreType.DMA((blocks,)),
         ],
         name="mixed",
-        compiler_params=room(60),
+        compiler_params=room(24),
         cost_estimate=cost(2 * rows * blocks * lanes * columns, 3_500_000),
-    )(gathered, weight)
+    )(pltpu.with_memory_space_constraint(gathered, pltpu.HBM), weight)
 
 
 def down_kernel(core_ref, early_ref, own_ref, other_ref, weight_ref, out_ref):

time: 152 us -> 151 us (level)
  Pallas kernels: 17 us -> 13.1 us
    pallas_call x1, Pallas kernels: 6.14 us -> 3.31 us  [hidden_of(): pl.pallas_call(functools.partial(hidden_kernel, blocks // 2), out_shape=j...]
    unnamed x14 -> x22, local copies, waits for them, and re-layouts: 4.14 us -> 5.38 us
where the time goes in v5:
time: 151 us; the launch traced here: 150 us
  blocking collectives  70.7 us (47%)
  starting transfers between devices  28.9 us (19%)
  waiting for transfers between devices  16.2 us (11%)
  between operations  14.2 us (9%)
  Pallas kernels  13.1 us (9%)
  local copies, waits for them, and re-layouts  6.09 us (4%)
    all_to_all x1, blocking collectives, shards(): lax.all_to_all(hidden, 'tp', 0, 0, tiled=True, axis_index_groups=columns_...  27.2 us
    all_gather x1, blocking collectives, shards(): early = lax.all_gather(arrived[:EARLY], 'tp', axis=0)  24.8 us
    all_gather x1, blocking collectives, shards(): early_hidden = lax.all_gather(early_hidden, 'tp', axis=0)  18.7 us
    all_to_all x1, starting transfers between devices, shards(): lax.all_to_all(outgoing, 'ep', 0, 0, tiled=True)  13.7 us
    all_to_all x1, starting transfers between devices, shards(): lax.all_to_all(produced.reshape(n_ep, capacity, produced.shape[1]), 'ep',...  9.02 us
    all_to_all x1, waiting for transfers between devices, shards(): lax.all_to_all(produced.reshape(n_ep, capacity, produced.shape[1]), 'ep',...  7.41 us
    unnamed x22, local copies, waits for them, and re-layouts  5.38 us
    all_to_all x1, waiting for transfers between devices, shards(): lax.all_to_all(outgoing, 'ep', 0, 0, tiled=True)  5.03 us
  transfers between devices with their start and end apart: 5, of which 5 were waited for; matrix products, arithmetic and copies ran while one was open for 1% of the time, Pallas kernels for 4%

profile of v5, /device:TPU:1, one launch (start us, length us, event | category | flops | bytes accessed | tf_op | source)
XLA Modules:
  0.0 150.1 jit_solution(16802165968203524017)
XLA Ops:
  7.2 0.0 copy-start.3
  7.2 0.0 copy-start.1
  7.2 2.1 %dispatch.1 = bf16[512,256]{1,0:T(8,128)(2,1)} custom-call(s32[2,128]{1,0:T(2,128)} %bitcast.19, bf16[128,256]{1,0:T(8,128)(2,1)} %rows_from.1), custom_call_target="tpu_custom_call" | custom-call | flops 50000000 | bytes 400000 | tf_op jit(solution)/shard_map/dispatch/pallas_call | solution.py:66
  9.3 13.7 %all-to-all-start = ((bf16[32,16,256]{2,1,0:T(8,128)(2,1)}), bf16[32,16,256]{2,1,0:T(8,128)(2,1)S(1)}, u32[]{:S(2)}, u32[]{:S(2)}) async-start(bf16[32,16,256]{2,1,0:T(8,128)(2,1)} %bitcast.25), calls=%async_computation | async-start | bytes 524288 | tf_op jit(solution)/shard_map/all_to_all | solution.py:321
  23.0 0.0 all-gather.4.cloned.1.call-start
  23.1 0.7 slice.15
  23.8 3.1 %collective-permute-start = (bf16[16,128]{1,0:T(8,128)(2,1)S(1)}, bf16[16,128]{1,0:T(8,128)(2,1)S(1)}, u32[]{:S(2)}, u32[]{:S(2)}) collective-permute-start(bf16[16,128]{1,0:T(8,128)(2,1)S(1)} %slice.15), channel_id=1, source_target_pairs={{0,16},{16,32},{32,48},{48,64},{64,80},{80,96},{96,112},{112,128},... | collective-permute-start | bytes 12296 | tf_op jit(solution)/shard_map/ppermute | solution.py:324
  26.9 0.1 pad_add_fusion.place_ref
  27.0 0.6 collective-permute-done.before_ref
  27.6 0.9 copy-done.6
  28.5 0.8 pool.1
  29.3 5.0 %all-to-all-done = bf16[32,16,256]{2,1,0:T(8,128)(2,1)S(1)} async-done(((bf16[32,16,256]{2,1,0:T(8,128)(2,1)}), bf16[32,16,256]{2,1,0:T(8,128)(2,1)S(1)}, u32[]{:S(2)}, u32[]{:S(2)}) %all-to-all-start) | async-done | bytes 262176 | tf_op jit(solution)/shard_map/all_to_all | solution.py:321
  34.3 0.8 pad_maximum_fusion
  35.1 0.0 all-gather.4.cloned.1.call-update
  35.1 24.8 %all_gather.21.rows_ref = bf16[16,112,256]{2,1,0:T(8,128)(2,1)S(1)} all-gather(bf16[1,112,256]{2,1,0:T(8,128)(2,1)S(1)} %bitcast.26), channel_id=1, replica_groups=mesh['ep'=32,'tp'=16] {'tp'}, dimensions={0}, use_global_device_ids=true | all-gather | bytes 974848 | tf_op jit(solution)/shard_map/all_gather | solution.py:334
  59.9 1.3 copy-done
  61.2 1.2 copy-done.2
  62.4 0.7 copy-done.7
  63.2 0.5 early_hidden.1
  63.6 18.7 %all-gather.1 = bf16[1792,128]{1,0:T(8,128)(2,1)S(1)} all-gather(bf16[112,128]{1,0:T(8,128)(2,1)S(1)} %early_hidden.1), channel_id=3, replica_groups=mesh['ep'=32,'tp'=16] {'tp'}, dimensions={0}, use_global_device_ids=true | all-gather | bytes 487424 | tf_op jit(solution)/shard_map/all_gather | solution.py:336
  82.3 1.2 all-gather.4.cloned.1.call-done
  83.5 3.3 %hidden.1 = bf16[8,400,128]{2,1,0:T(8,128)(2,1)S(1)} custom-call(bf16[16,1312,128]{2,1,0:T(8,128)(2,1)} %bitcast.22, f32[1,4096]{1,0:T(1,128)S(1)} %bitcast.18, bf16[1,4096,128]{2,1,0:T(8,128)(2,1)S(1)} %copy-done.1, bf16[1,4096,128]{2,1,0:T(8,128)(2,1)S(1)} %copy-done.3), custom_call_target="tpu_custom_call" | custom-call | flops 838860800 | bytes 6500000 | tf_op jit(solution)/shard_map/hidden/pallas_call | solution.py:226
  86.9 27.2 %all_to_all.15.own_ref = bf16[8,400,128]{2,1,0:T(8,128)(2,1)S(1)} all-to-all(bf16[8,400,128]{2,1,0:T(8,128)(2,1)S(1)} %hidden.1), channel_id=1, replica_groups={{0,2,4,6,8,10,12,14},{1,3,5,7,9,11,13,15},{16,18,20,22,24,26,28,30},{17..., dimensions={0} | all-to-all | bytes 1638400 | tf_op jit(solution)/shard_map/all_to_all | solution.py:343
  114.1 3.0 %collective-permute-start.1 = (bf16[8,400,128]{2,1,0:T(8,128)(2,1)S(1)}, bf16[8,400,128]{2,1,0:T(8,128)(2,1)S(1)}, u32[]{:S(2)}, u32[]{:S(2)}) collective-permute-start(bf16[8,400,128]{2,1,0:T(8,128)(2,1)S(1)} %all_to_all.15.own_ref), channel_id=1, source_target_pairs={{0,1},{1,0},{2,3},{3,2},{4,5},{5,4},{6,7},{7,6},{8,9},{9,8},{10,11... | collective-permute-start | bytes 2457608 | tf_op jit(solution)/shard_map/ppermute | solution.py:344
  117.1 1.9 %collective-permute-done.1.other_ref = bf16[8,400,128]{2,1,0:T(8,128)(2,1)S(1)} collective-permute-done((bf16[8,400,128]{2,1,0:T(8,128)(2,1)S(1)}, bf16[8,400,128]{2,1,0:T(8,128)(2,1)S(1)}, u32[]{:S(2)}, u32[]{:S(2)}) %collective-permute-start.1) | collective-permute-done | bytes 819232 | tf_op jit(solution)/shard_map/ppermute | solution.py:344
  119.1 1.2 copy-done.5
  120.3 1.5 down.1
  121.7 9.0 %all-to-all-start.2 = ((bf16[32,16,256]{2,1,0:T(8,128)(2,1)}), bf16[32,16,256]{2,1,0:T(8,128)(2,1)S(1)}, u32[]{:S(2)}, u32[]{:S(2)}) async-start(bf16[32,16,256]{2,1,0:T(8,128)(2,1)} %bitcast.12), calls=%async_computation.2 | async-start | bytes 524288 | tf_op jit(solution)/shard_map/all_to_all | solution.py:350
  130.8 0.5 shares.1
  131.3 3.6 %mixed.1 = bf16[512,256]{1,0:T(8,128)(2,1)} custom-call(bf16[16,1312,128]{2,1,0:T(8,128)(2,1)} %bitcast.23, bf16[2048,256]{1,0:T(8,128)(2,1)S(1)} %copy-done.4), custom_call_target="tpu_custom_call" | custom-call | flops 536870912 | bytes 3500000 | tf_op jit(solution)/shard_map/mixed/pallas_call | solution.py:258
  134.9 7.4 %all-to-all-done.2 = bf16[32,16,256]{2,1,0:T(8,128)(2,1)S(1)} async-done(((bf16[32,16,256]{2,1,0:T(8,128)(2,1)}), bf16[32,16,256]{2,1,0:T(8,128)(2,1)S(1)}, u32[]{:S(2)}, u32[]{:S(2)}) %all-to-all-start.2) | async-done | bytes 262176 | tf_op jit(solution)/shard_map/all_to_all | solution.py:350
  142.4 0.9 combine.1
  (17 shorter events, 0.1 us)
Async XLA Ops:
  7.2 76.3 %copy-start.3 = (bf16[1,4096,128]{2,1,0:T(8,128)(2,1)S(1)}, bf16[1,4096,128]{2,1,0:T(8,128)(2,1)}, u32[]{:S(2)}) copy-start(bf16[1,4096,128]{2,1,0:T(8,128)(2,1)} %up_ref.3) | copy-start | bytes 3145732
  7.2 76.3 %copy-start.1 = (bf16[1,4096,128]{2,1,0:T(8,128)(2,1)S(1)}, bf16[1,4096,128]{2,1,0:T(8,128)(2,1)}, u32[]{:S(2)}) copy-start(bf16[1,4096,128]{2,1,0:T(8,128)(2,1)} %gate_ref.3) | copy-start | bytes 3145732
  9.3 25.0 %all-to-all-start = ((bf16[32,16,256]{2,1,0:T(8,128)(2,1)}), bf16[32,16,256]{2,1,0:T(8,128)(2,1)S(1)}, u32[]{:S(2)}, u32[]{:S(2)}) async-start(bf16[32,16,256]{2,1,0:T(8,128)(2,1)} %bitcast.25), calls=%async_computation | async-start | bytes 524288 | tf_op jit(solution)/shard_map/all_to_all | solution.py:321
  23.0 60.5 %all-gather.4.cloned.1.call-start = ((), (), s32[]{:S(2)}) async-start(), calls=%async_computation.3 | async-start | bytes 5709824 | tf_op jit(solution)/shard_map/all_gather | solution.py:333
  23.8 3.9 %collective-permute-start = (bf16[16,128]{1,0:T(8,128)(2,1)S(1)}, bf16[16,128]{1,0:T(8,128)(2,1)S(1)}, u32[]{:S(2)}, u32[]{:S(2)}) collective-permute-start(bf16[16,128]{1,0:T(8,128)(2,1)S(1)} %slice.15), channel_id=1, source_target_pairs={{0,16},{16,32},{32,48},{48,64},{64,80},{80,96},{96,112},{112,128},... | collective-permute-start | bytes 12296 | tf_op jit(solution)/shard_map/ppermute | solution.py:324
  27.6 0.9 copy-start.6
  28.5 55.0 %copy-start.8 = (f32[4096]{0:T(1024)S(1)}, f32[4096]{0:T(1024)}, u32[]{:S(2)}) copy-start(f32[4096]{0:T(1024)} %param.14) | copy-start | bytes 49156
  59.9 1.3 copy-start
  61.2 1.2 copy-start.2
  62.4 0.7 copy-start.7
  83.5 47.3 %copy-start.9 = (s32[128,2]{0,1:T(2,128)S(1)}, s32[128,2]{0,1:T(2,128)}, u32[]{:S(2)}) copy-start(s32[128,2]{0,1:T(2,128)} %param.12) | copy-start | bytes 3076
  83.5 47.3 %copy-start.10 = (f32[128,2]{0,1:T(2,128)S(1)}, f32[128,2]{0,1:T(2,128)}, u32[]{:S(2)}) copy-start(f32[128,2]{0,1:T(2,128)} %param.13) | copy-start | bytes 3076
  86.9 44.4 %copy-start.4 = (bf16[2048,256]{1,0:T(8,128)(2,1)S(1)}, bf16[2048,256]{1,0:T(8,128)(2,1)}, u32[]{:S(2)}) copy-start(bf16[2048,256]{1,0:T(8,128)(2,1)} %weight_ref.1) | copy-start | bytes 3145732
  114.1 4.9 %collective-permute-start.1 = (bf16[8,400,128]{2,1,0:T(8,128)(2,1)S(1)}, bf16[8,400,128]{2,1,0:T(8,128)(2,1)S(1)}, u32[]{:S(2)}, u32[]{:S(2)}) collective-permute-start(bf16[8,400,128]{2,1,0:T(8,128)(2,1)S(1)} %all_to_all.15.own_ref), channel_id=1, source_target_pairs={{0,1},{1,0},{2,3},{3,2},{4,5},{5,4},{6,7},{7,6},{8,9},{9,8},{10,11... | collective-permute-start | bytes 2457608 | tf_op jit(solution)/shard_map/ppermute | solution.py:344
  119.1 1.2 copy-start.5
  121.7 20.6 %all-to-all-start.2 = ((bf16[32,16,256]{2,1,0:T(8,128)(2,1)}), bf16[32,16,256]{2,1,0:T(8,128)(2,1)S(1)}, u32[]{:S(2)}, u32[]{:S(2)}) async-start(bf16[32,16,256]{2,1,0:T(8,128)(2,1)} %bitcast.12), calls=%async_computation.2 | async-start | bytes 524288 | tf_op jit(solution)/shard_map/all_to_all | solution.py:350
Sparse Core Ops, SparseCore 0:
  35.3 48.2 all-gather.3

commit v6 on v5

--- a/solution.py
+++ b/solution.py
@@ -16,7 +16,7 @@
 VMEM = pl.BlockSpec(memory_space=pltpu.VMEM)
 SMEM = pl.BlockSpec(memory_space=pltpu.SMEM)
 HBM = pl.BlockSpec(memory_space=pltpu.HBM)
-EARLY = 112
+EARLY = 120
 
 
 def room(mib):

time: 151 us -> 150 us (level)
  no operation moved by 1% of the time
where the time goes in v6:
time: 150 us; the launch traced here: 149 us
  blocking collectives  71.8 us (48%)
  starting transfers between devices  27.8 us (19%)
  waiting for transfers between devices  15.8 us (11%)
  between operations  14.2 us (9%)
  Pallas kernels  13.1 us (9%)
  local copies, waits for them, and re-layouts  6.07 us (4%)
    all_to_all x1, blocking collectives, shards(): lax.all_to_all(hidden, 'tp', 0, 0, tiled=True, axis_index_groups=columns_...  27.3 us
    all_gather x1, blocking collectives, shards(): early = lax.all_gather(arrived[:EARLY], 'tp', axis=0)  25.1 us
    all_gather x1, blocking collectives, shards(): early_hidden = lax.all_gather(early_hidden, 'tp', axis=0)  19.4 us
    all_to_all x1, starting transfers between devices, shards(): lax.all_to_all(outgoing, 'ep', 0, 0, tiled=True)  13.7 us
    all_to_all x1, starting transfers between devices, shards(): lax.all_to_all(produced.reshape(n_ep, capacity, produced.shape[1]), 'ep',...  8.36 us
    all_to_all x1, waiting for transfers between devices, shards(): lax.all_to_all(produced.reshape(n_ep, capacity, produced.shape[1]), 'ep',...  7.41 us
    unnamed x22, local copies, waits for them, and re-layouts  5.35 us
    all_to_all x1, waiting for transfers between devices, shards(): lax.all_to_all(outgoing, 'ep', 0, 0, tiled=True)  5.03 us
  transfers between devices with their start and end apart: 5, of which 5 were waited for; matrix products, arithmetic and copies ran while one was open for 1% of the time, Pallas kernels for 4%

profile of v6, /device:TPU:1, one launch (start us, length us, event | category | flops | bytes accessed | tf_op | source)
XLA Modules:
  0.0 149.5 jit_solution(6896734400132465787)
XLA Ops:
  7.2 0.0 copy-start.3
  7.2 0.0 copy-start.1
  7.2 2.1 %dispatch.1 = bf16[512,256]{1,0:T(8,128)(2,1)} custom-call(s32[2,128]{1,0:T(2,128)} %bitcast.20, bf16[128,256]{1,0:T(8,128)(2,1)} %rows_from.1), custom_call_target="tpu_custom_call" | custom-call | flops 50000000 | bytes 400000 | tf_op jit(solution)/shard_map/dispatch/pallas_call | solution.py:66
  9.3 13.7 %all-to-all-start = ((bf16[32,16,256]{2,1,0:T(8,128)(2,1)}), bf16[32,16,256]{2,1,0:T(8,128)(2,1)S(1)}, u32[]{:S(2)}, u32[]{:S(2)}) async-start(bf16[32,16,256]{2,1,0:T(8,128)(2,1)} %bitcast.25), calls=%async_computation | async-start | bytes 524288 | tf_op jit(solution)/shard_map/all_to_all | solution.py:321
  23.0 0.0 all-gather.5.cloned.1.call-start
  23.1 0.7 slice.14
  23.8 3.1 %collective-permute-start = (bf16[16,128]{1,0:T(8,128)(2,1)S(1)}, bf16[16,128]{1,0:T(8,128)(2,1)S(1)}, u32[]{:S(2)}, u32[]{:S(2)}) collective-permute-start(bf16[16,128]{1,0:T(8,128)(2,1)S(1)} %slice.14), channel_id=1, source_target_pairs={{0,16},{16,32},{32,48},{48,64},{64,80},{80,96},{96,112},{112,128},... | collective-permute-start | bytes 12296 | tf_op jit(solution)/shard_map/ppermute | solution.py:324
  26.9 0.1 pad_add_fusion.place_ref
  27.0 0.6 collective-permute-done.before_ref
  27.6 0.9 copy-done.6
  28.5 0.8 pool.1
  29.3 5.0 %all-to-all-done = bf16[32,16,256]{2,1,0:T(8,128)(2,1)S(1)} async-done(((bf16[32,16,256]{2,1,0:T(8,128)(2,1)}), bf16[32,16,256]{2,1,0:T(8,128)(2,1)S(1)}, u32[]{:S(2)}, u32[]{:S(2)}) %all-to-all-start) | async-done | bytes 262176 | tf_op jit(solution)/shard_map/all_to_all | solution.py:321
  34.3 0.8 pad_maximum_fusion
  35.1 0.0 all-gather.5.cloned.1.call-update
  35.2 25.1 %all-gather.1 = bf16[1920,256]{1,0:T(8,128)(2,1)S(1)} all-gather(bf16[120,256]{1,0:T(8,128)(2,1)S(1)} %slice.18), channel_id=3, replica_groups=mesh['ep'=32,'tp'=16] {'tp'}, dimensions={0}, use_global_device_ids=true | all-gather | bytes 1044480 | tf_op jit(solution)/shard_map/all_gather | solution.py:334
  60.2 1.2 copy-done
  61.5 1.2 copy-done.2
  62.7 0.7 copy-done.7
  63.4 0.5 early_hidden.1
  63.9 19.4 %all-gather.2 = bf16[1920,128]{1,0:T(8,128)(2,1)S(1)} all-gather(bf16[120,128]{1,0:T(8,128)(2,1)S(1)} %early_hidden.1), channel_id=4, replica_groups=mesh['ep'=32,'tp'=16] {'tp'}, dimensions={0}, use_global_device_ids=true | all-gather | bytes 522240 | tf_op jit(solution)/shard_map/all_gather | solution.py:336
  83.3 0.8 all-gather.5.cloned.1.call-done
  84.1 3.3 %hidden.1 = bf16[8,392,128]{2,1,0:T(8,128)(2,1)S(1)} custom-call(bf16[16,1296,128]{2,1,0:T(8,128)(2,1)} %bitcast.23, f32[1,4096]{1,0:T(1,128)S(1)} %bitcast.19, bf16[1,4096,128]{2,1,0:T(8,128)(2,1)S(1)} %copy-done.1, bf16[1,4096,128]{2,1,0:T(8,128)(2,1)S(1)} %copy-done.3), custom_call_target="tpu_custom_call" | custom-call | flops 822083584 | bytes 6500000 | tf_op jit(solution)/shard_map/hidden/pallas_call | solution.py:226
  87.4 27.3 %all_to_all.15.own_ref = bf16[8,392,128]{2,1,0:T(8,128)(2,1)S(1)} all-to-all(bf16[8,392,128]{2,1,0:T(8,128)(2,1)S(1)} %hidden.1), channel_id=1, replica_groups={{0,2,4,6,8,10,12,14},{1,3,5,7,9,11,13,15},{16,18,20,22,24,26,28,30},{17..., dimensions={0} | all-to-all | bytes 1605632 | tf_op jit(solution)/shard_map/all_to_all | solution.py:343
  114.7 2.5 %collective-permute-start.1 = (bf16[8,392,128]{2,1,0:T(8,128)(2,1)S(1)}, bf16[8,392,128]{2,1,0:T(8,128)(2,1)S(1)}, u32[]{:S(2)}, u32[]{:S(2)}) collective-permute-start(bf16[8,392,128]{2,1,0:T(8,128)(2,1)S(1)} %all_to_all.15.own_ref), channel_id=1, source_target_pairs={{0,1},{1,0},{2,3},{3,2},{4,5},{5,4},{6,7},{7,6},{8,9},{9,8},{10,11... | collective-permute-start | bytes 2408456 | tf_op jit(solution)/shard_map/ppermute | solution.py:344
  117.2 1.9 %collective-permute-done.1.other_ref = bf16[8,392,128]{2,1,0:T(8,128)(2,1)S(1)} collective-permute-done((bf16[8,392,128]{2,1,0:T(8,128)(2,1)S(1)}, bf16[8,392,128]{2,1,0:T(8,128)(2,1)S(1)}, u32[]{:S(2)}, u32[]{:S(2)}) %collective-permute-start.1) | collective-permute-done | bytes 802848 | tf_op jit(solution)/shard_map/ppermute | solution.py:344
  119.1 1.2 copy-done.5
  120.4 1.5 down.1
  121.8 8.4 %all-to-all-start.2 = ((bf16[32,16,256]{2,1,0:T(8,128)(2,1)}), bf16[32,16,256]{2,1,0:T(8,128)(2,1)S(1)}, u32[]{:S(2)}, u32[]{:S(2)}) async-start(bf16[32,16,256]{2,1,0:T(8,128)(2,1)} %bitcast.12), calls=%async_computation.2 | async-start | bytes 524288 | tf_op jit(solution)/shard_map/all_to_all | solution.py:350
  130.2 0.5 shares.1
  130.7 3.6 %mixed.1 = bf16[512,256]{1,0:T(8,128)(2,1)} custom-call(bf16[16,1296,128]{2,1,0:T(8,128)(2,1)} %bitcast.24, bf16[2048,256]{1,0:T(8,128)(2,1)S(1)} %copy-done.4), custom_call_target="tpu_custom_call" | custom-call | flops 536870912 | bytes 3500000 | tf_op jit(solution)/shard_map/mixed/pallas_call | solution.py:258
  134.4 7.4 %all-to-all-done.2 = bf16[32,16,256]{2,1,0:T(8,128)(2,1)S(1)} async-done(((bf16[32,16,256]{2,1,0:T(8,128)(2,1)}), bf16[32,16,256]{2,1,0:T(8,128)(2,1)S(1)}, u32[]{:S(2)}, u32[]{:S(2)}) %all-to-all-start.2) | async-done | bytes 262176 | tf_op jit(solution)/shard_map/all_to_all | solution.py:350
  141.8 0.9 combine.1
  (17 shorter events, 0.1 us)
Async XLA Ops:
  7.2 76.9 %copy-start.3 = (bf16[1,4096,128]{2,1,0:T(8,128)(2,1)S(1)}, bf16[1,4096,128]{2,1,0:T(8,128)(2,1)}, u32[]{:S(2)}) copy-start(bf16[1,4096,128]{2,1,0:T(8,128)(2,1)} %up_ref.3) | copy-start | bytes 3145732
  7.2 76.9 %copy-start.1 = (bf16[1,4096,128]{2,1,0:T(8,128)(2,1)S(1)}, bf16[1,4096,128]{2,1,0:T(8,128)(2,1)}, u32[]{:S(2)}) copy-start(bf16[1,4096,128]{2,1,0:T(8,128)(2,1)} %gate_ref.3) | copy-start | bytes 3145732
  9.3 25.0 %all-to-all-start = ((bf16[32,16,256]{2,1,0:T(8,128)(2,1)}), bf16[32,16,256]{2,1,0:T(8,128)(2,1)S(1)}, u32[]{:S(2)}, u32[]{:S(2)}) async-start(bf16[32,16,256]{2,1,0:T(8,128)(2,1)} %bitcast.25), calls=%async_computation | async-start | bytes 524288 | tf_op jit(solution)/shard_map/all_to_all | solution.py:321
  23.0 61.0 %all-gather.5.cloned.1.call-start = ((), (), s32[]{:S(2)}) async-start(), calls=%async_computation.3 | async-start | bytes 5640192 | tf_op jit(solution)/shard_map/all_gather | solution.py:333
  23.8 3.9 %collective-permute-start = (bf16[16,128]{1,0:T(8,128)(2,1)S(1)}, bf16[16,128]{1,0:T(8,128)(2,1)S(1)}, u32[]{:S(2)}, u32[]{:S(2)}) collective-permute-start(bf16[16,128]{1,0:T(8,128)(2,1)S(1)} %slice.14), channel_id=1, source_target_pairs={{0,16},{16,32},{32,48},{48,64},{64,80},{80,96},{96,112},{112,128},... | collective-permute-start | bytes 12296 | tf_op jit(solution)/shard_map/ppermute | solution.py:324
  27.6 0.9 copy-start.6
  28.5 55.5 %copy-start.8 = (f32[4096]{0:T(1024)S(1)}, f32[4096]{0:T(1024)}, u32[]{:S(2)}) copy-start(f32[4096]{0:T(1024)} %param.14) | copy-start | bytes 49156
  60.2 1.2 copy-start
  61.5 1.2 copy-start.2
  62.7 0.7 copy-start.7
  84.0 46.1 %copy-start.9 = (s32[128,2]{0,1:T(2,128)S(1)}, s32[128,2]{0,1:T(2,128)}, u32[]{:S(2)}) copy-start(s32[128,2]{0,1:T(2,128)} %param.12) | copy-start | bytes 3076
  84.1 46.2 %copy-start.10 = (f32[128,2]{0,1:T(2,128)S(1)}, f32[128,2]{0,1:T(2,128)}, u32[]{:S(2)}) copy-start(f32[128,2]{0,1:T(2,128)} %param.13) | copy-start | bytes 3076
  87.4 43.4 %copy-start.4 = (bf16[2048,256]{1,0:T(8,128)(2,1)S(1)}, bf16[2048,256]{1,0:T(8,128)(2,1)}, u32[]{:S(2)}) copy-start(bf16[2048,256]{1,0:T(8,128)(2,1)} %weight_ref.1) | copy-start | bytes 3145732
  114.7 4.4 %collective-permute-start.1 = (bf16[8,392,128]{2,1,0:T(8,128)(2,1)S(1)}, bf16[8,392,128]{2,1,0:T(8,128)(2,1)S(1)}, u32[]{:S(2)}, u32[]{:S(2)}) collective-permute-start(bf16[8,392,128]{2,1,0:T(8,128)(2,1)S(1)} %all_to_all.15.own_ref), channel_id=1, source_target_pairs={{0,1},{1,0},{2,3},{3,2},{4,5},{5,4},{6,7},{7,6},{8,9},{9,8},{10,11... | collective-permute-start | bytes 2408456 | tf_op jit(solution)/shard_map/ppermute | solution.py:344
  119.1 1.2 copy-start.5
  121.8 20.0 %all-to-all-start.2 = ((bf16[32,16,256]{2,1,0:T(8,128)(2,1)}), bf16[32,16,256]{2,1,0:T(8,128)(2,1)S(1)}, u32[]{:S(2)}, u32[]{:S(2)}) async-start(bf16[32,16,256]{2,1,0:T(8,128)(2,1)} %bitcast.12), calls=%async_computation.2 | async-start | bytes 524288 | tf_op jit(solution)/shard_map/all_to_all | solution.py:350
Sparse Core Ops, SparseCore 0:
  35.3 48.7 all-gather.4
